TPU v7x, 32 devices: a whole 2x2x4 slice. The times are simulated.
32 devices in a mesh: sp: 4 (over z), fs: 4 (over y, x), tp: 2 (over core).
Axes of the slice: x: 2, y: 2, z: 4, core: 2. Of those that a mesh axis runs over, the one named last changes fastest.
Arguments:
- tokens: bfloat16 [4, 512, 2048], P('fs', ('sp', 'tp')), may hold values from -6 to 6
- norm_gain: float32 [2048], replicated, may hold values from 0.1 to 1.9
- gla_query_weight: bfloat16 [2048, 512], P('sp', 'tp'), may hold values from -0.125 to 0.125
- gla_key_weight: bfloat16 [2048, 512], P('sp', 'tp'), may hold values from -0.125 to 0.125
- gla_value_weight: bfloat16 [2048, 1024], P('sp', 'tp'), may hold values from -0.125 to 0.125
- decay_down: bfloat16 [2048, 32], P('sp'), may hold values from -0.125 to 0.125
- decay_up: bfloat16 [32, 512], P(None, 'tp'), may hold values from -1 to 1
- decay_bias: float32 [512], P('tp'), may hold values from 0.5 to 12
- head_gain: float32 [128], replicated, may hold values from 0.1 to 1.9
- window_query_weight: bfloat16 [2048, 1024], P('sp', 'tp'), may hold values from -3 to 3
- window_key_weight: bfloat16 [2048, 256], P('sp', 'tp'), may hold values from -3 to 3
- window_value_weight: bfloat16 [2048, 256], P('sp', 'tp'), may hold values from -0.125 to 0.125
- sink_logit: float32 [16], P('tp'), may hold values from 3 to 7
- gla_output_weight: bfloat16 [1024, 2048], P('tp', 'sp'), may hold values from -0.125 to 0.125
- window_output_weight: bfloat16 [1024, 2048], P('tp', 'sp'), may hold values from -0.125 to 0.125
Outputs:
- mixed: bfloat16 [4, 512, 2048], P('fs', ('sp', 'tp'))
All inputs are finite; a program needn't handle non-finite values.
Results may differ from a plain program's by a relative error of at most 0.013.
Values may be sent and summed in bfloat16 or wider, within the bound.
A program may use at most 64 MiB of HBM per device.

v0:
```python
import functools

import jax
import jax.numpy as jnp
from jax import lax
from jax.experimental import pallas as pl
from jax.experimental.pallas import tpu as pltpu
from jax.sharding import PartitionSpec as P

KEY_DIM = 64
VALUE_DIM = 128
SWA_HEADS = 16
KV_HEADS = 4
HEAD_DIM = 64
WINDOW = 128
SPAN = 64

EPS = 1e-06
SOFTMAX_TEMPER = 16.0
BF = jnp.bfloat16
F32 = jnp.float32


def rms_rows(values, gain):
    mean_square = jnp.mean(values * values, axis=-1, keepdims=True)
    return values * lax.rsqrt(mean_square + EPS) * gain


def nt(a, b):
    return lax.dot_general(a, b, (((1,), (1,)), ((), ())), preferred_element_type=F32)


def nn(a, b):
    return lax.dot_general(a, b, (((1,), (0,)), ((), ())), preferred_element_type=F32)


def tn(a, b):
    return lax.dot_general(a, b, (((0,), (0,)), ((), ())), preferred_element_type=F32)


def exact(a, b):
    return lax.dot_general(
        a, b, (((1,), (0,)), ((), ())), precision=lax.Precision.HIGHEST, preferred_element_type=F32
    )


def mixer_kernel(
    sizes,
    tok_ref,
    gv_ref,
    wq_ref,
    gq_ref,
    gk_ref,
    wk_ref,
    wv_ref,
    low_ref,
    go_ref,
    wo_ref,
    ngain_ref,
    up_ref,
    bias_ref,
    hgain_ref,
    sink_ref,
    out_ref,
    x_buf,
    w_buf,
    l_buf,
    o_buf,
    proj,
    edge_out,
    edge_in,
    state_out,
    state_in,
    local_out,
    q_far,
    hidden,
    half_out,
    half_in,
    half_own,
    piece_out,
    piece_in,
    piece_own,
    local_sem,
    tok_send,
    tok_recv,
    w_send,
    w_recv,
    l_send,
    l_recv,
    v_send,
    v_recv,
    vp_send,
    vp_recv,
    lp_send,
    lp_recv,
    o_send,
    o_recv,
    edge_sem,
    state_send,
    state_recv,
    half_send,
    half_recv,
    piece_send,
    piece_recv,
):
    sp, fs, tp = sizes
    me = lax.axis_index("sp")
    f = lax.axis_index("fs")
    c = lax.axis_index("tp")
    plane = fs * tp
    mine = f * tp + c
    own = tok_ref.shape[0]
    rows = own * tp
    kc = gv_ref.shape[0]
    MESH = pl.DeviceIdType.MESH

    def remote(src, dst, ssem, rsem, target):
        return pltpu.make_async_remote_copy(
            src_ref=src, dst_ref=dst, send_sem=ssem, recv_sem=rsem,
            device_id=target, device_id_type=MESH,
        )

    def w_rows(s):
        return w_buf.at[pl.ds(pl.multiple_of(s * kc, kc), kc)]

    def w_copy(s, way, first):
        target = {"sp": me + (1 if way == 0 else -1)}
        return remote(
            w_main(s), w_main(s), w_send.at[way, s], w_recv.at[s], target
        )

    side = f % 2
    part = kc // 2
    lpart = low_ref.shape[0] // 2

    def w_main(s):
        return w_rows(s).at[:, : starts[4]]

    def v_rows(s, h):
        at = pl.multiple_of(s * kc + h * part, part)
        return w_buf.at[pl.ds(at, part), starts[4] : starts[4] + 2 * HEAD_DIM]

    def l_rows(s, h):
        return l_buf.at[s, pl.ds(pl.multiple_of(h * lpart, lpart), lpart)]

    def v_copy(s, way):
        target = {"sp": me + (1 if way == 0 else -1)}
        return remote(v_rows(s, side), v_rows(s, side), v_send.at[way, s], v_recv.at[s], target)

    def lh_copy(s, way):
        target = {"sp": me + (1 if way == 0 else -1)}
        return remote(l_rows(s, side), l_rows(s, side), l_send.at[way, s], l_recv.at[s], target)

    def pair_copies(s, h):
        target = {"fs": f + 1 - 2 * side}
        return (
            remote(v_rows(s, h), v_rows(s, h), vp_send.at[s], vp_recv.at[s], target),
            remote(l_rows(s, h), l_rows(s, h), lp_send.at[s], lp_recv.at[s], target),
        )

    class l_copy:
        def __init__(self, s, way, first):
            self.s = s
            self.both = (v_copy(s, way), lh_copy(s, way))

        def start(self):
            for copy in self.both:
                copy.start()

        def wait_recv(self):
            for copy, onward in zip(self.both, pair_copies(self.s, side)):
                copy.wait_recv()
                onward.start()

        def wait_send(self):
            for copy in self.both:
                copy.wait_send()

    def o_copy(s, way, first):
        target = {"sp": me + (1 if way == 0 else -1)}
        return remote(
            o_buf.at[s], o_buf.at[s], o_send.at[way, s], o_recv.at[s], target
        )

    def tok_rows(i):
        return x_buf.at[pl.ds(pl.multiple_of(i * own, own), own)]

    def tok_copy(d, peer, sender):
        return remote(
            tok_ref, tok_rows(sender), tok_send.at[d - 1], tok_recv.at[d - 1],
            {"fs": peer // tp, "tp": peer % tp},
        )

    def pick(ref, width, which):
        value = ref[:, :width]
        for i in range(1, ref.shape[1] // width):
            value = jnp.where(which == i, ref[:, i * width : (i + 1) * width], value)
        return value

    def lanes(ref, width):
        return ref.at[:, pl.ds(pl.multiple_of(f * width, width), width)]

    def depth(ref, width):
        return ref.at[pl.ds(pl.multiple_of(f * width, width), width)]

    cols = [VALUE_DIM, 2 * HEAD_DIM, KEY_DIM, KEY_DIM, HEAD_DIM, HEAD_DIM]
    starts = [sum(cols[:i]) for i in range(len(cols))]
    gd = go_ref.shape[0] // fs
    wd = wo_ref.shape[0] // fs
    heads = sink_ref.shape[1] // fs
    copies_in = [
        (lanes(gv_ref, cols[0]), w_rows(me).at[:, : cols[0]]),
        (lanes(wq_ref, cols[1]), w_rows(me).at[:, starts[1] : starts[2]]),
        (depth(go_ref, gd), o_buf.at[me, pl.ds(0, gd)]),
        (depth(wo_ref, wd), o_buf.at[me, pl.ds(gd, wd)]),
        (low_ref, l_buf.at[me]),
        (tok_ref, tok_rows(mine)),
    ]
    locals_ = [
        pltpu.make_async_copy(a, b, local_sem.at[i]) for i, (a, b) in enumerate(copies_in)
    ]
    for copy in locals_:
        copy.start()
    for d in range(1, plane):
        tok_copy(d, lax.rem(mine + d, plane), mine).start()
    own_rows = pl.ds(pl.multiple_of(me * kc, kc), kc)
    kv = (f * heads) // (SWA_HEADS // KV_HEADS)
    w_buf[own_rows, starts[2] : starts[4]] = jnp.concatenate(
        [pick(gq_ref, KEY_DIM, f), pick(gk_ref, KEY_DIM, f)], 1
    )
    w_buf[own_rows, starts[4] :] = jnp.concatenate(
        [pick(wk_ref, HEAD_DIM, kv), pick(wv_ref, HEAD_DIM, kv)], 1
    )
    for copy in locals_[:5]:
        copy.wait()

    def sends(k):
        @pl.when((me - k >= 0) & (me + 1 < sp))
        def _():
            l_copy(me - k, 0, k == 0).start()
            w_copy(me - k, 0, k == 0).start()

        @pl.when((me + k < sp) & (me >= 1))
        def _():
            l_copy(me + k, 1, k == 0).start()
            w_copy(me + k, 1, k == 0).start()

        @pl.when((me == k) & (me + 1 < sp))
        def _():
            o_copy(me, 0, True).start()

        @pl.when((sp - 1 - me == k) & (me >= 1))
        def _():
            o_copy(me, 1, True).start()

    for k in range(sp - 1):
        sends(k)

        @pl.when(me - 1 - k >= 0)
        def _():
            l_copy(me - 1 - k, 0, False).wait_recv()
            w_copy(me - 1 - k, 0, False).wait_recv()

        @pl.when(me + 1 + k < sp)
        def _():
            l_copy(me + 1 + k, 1, False).wait_recv()
            w_copy(me + 1 + k, 1, False).wait_recv()

    inner = (me >= 1) & (me + 1 < sp)
    for k in range(1, sp - 1):
        @pl.when(inner & (me - k >= 0))
        def _():
            o_copy(me - k, 0, False).wait_recv()
            o_copy(me - k, 0, False).start()

        @pl.when(inner & (me + k < sp))
        def _():
            o_copy(me + k, 1, False).wait_recv()
            o_copy(me + k, 1, False).start()

    for copy in locals_[5:]:
        copy.wait()
    for i in range(sp):
        @pl.when(i != me)
        def _():
            for copy in pair_copies(i, 1 - side):
                copy.wait_recv()

    for d in range(1, plane):
        tok_copy(d, mine, lax.rem(mine + plane - d, plane)).wait_recv()


    def project(b, _):
        x = x_buf[pl.ds(pl.multiple_of(b * rows, rows), rows)].astype(F32)
        normed = rms_rows(x, ngain_ref[...]).astype(BF)
        p = nn(normed, w_buf[...]).astype(BF)
        proj[b, :, : p.shape[1]] = p
        edge_out[b] = p[rows - WINDOW :, starts[4] : starts[4] + 2 * HEAD_DIM]
        low = nt(normed[:, :kc], l_buf[0])
        for s in range(1, sp):
            low += nt(normed[:, s * kc : (s + 1) * kc], l_buf[s])
        proj[b, :, p.shape[1] : p.shape[1] + low.shape[1]] = low.astype(BF)
        return 0

    lax.fori_loop(0, fs, project, 0)
    edge = remote(edge_out, edge_in, edge_sem.at[0], edge_sem.at[1], {"sp": me + 1})

    @pl.when(me + 1 < sp)
    def _():
        edge.start()

    @pl.when(me == 0)
    def _():
        edge_in[...] = jnp.zeros_like(edge_in)

    nb = rows // SPAN
    low_at = sum(cols)
    lower = (
        lax.broadcasted_iota(jnp.int32, (SPAN, SPAN), 0)
        >= lax.broadcasted_iota(jnp.int32, (SPAN, SPAN), 1)
    )
    tri = lower.astype(F32)
    up = pick(up_ref, KEY_DIM, f)
    bias = pick(bias_ref, KEY_DIM, f)
    sinks = pick(sink_ref, heads, f)
    for b in range(fs):
        low = proj[b, :, low_at : low_at + up_ref.shape[0]]
        z = nn(low, up) + bias
        rate = (jnp.minimum(z, 0.0) - jnp.log1p(jnp.exp(-jnp.abs(z)))) / SOFTMAX_TEMPER
        state = None
        before = jnp.zeros((1, KEY_DIM), F32)
        for n in range(nb):
            r0 = n * SPAN
            within = exact(tri, rate[r0 : r0 + SPAN])
            total = within[SPAN - 1 :]
            v = proj[b, r0 : r0 + SPAN, starts[0] : starts[0] + VALUE_DIM]
            q = proj[b, r0 : r0 + SPAN, starts[2] : starts[2] + KEY_DIM].astype(F32)
            k = proj[b, r0 : r0 + SPAN, starts[3] : starts[3] + KEY_DIM].astype(F32)
            q_dec = q * KEY_DIM**-0.5 * jnp.exp(within)
            k_dec = (k * jnp.exp(-within)).astype(BF)
            k_end = (k * jnp.exp(total - within)).astype(BF)
            scores = jnp.where(lower, nt(q_dec.astype(BF), k_dec), 0.0)
            o = nn(scores.astype(BF), v)
            if state is not None:
                o += nt(q_dec.astype(BF), state.astype(BF))
            local_out[b, r0 : r0 + SPAN] = o
            q_far[b, r0 : r0 + SPAN] = (q_dec * jnp.exp(before)).astype(BF)
            update = tn(v, k_end)
            state = update if state is None else jnp.exp(total) * state + update
            before = before + total
        half = (b % 2) * KEY_DIM
        state_out[b // 2, :VALUE_DIM, half : half + KEY_DIM] = state.astype(BF)
        state_out[b // 2, VALUE_DIM:, half : half + KEY_DIM] = jnp.broadcast_to(
            jnp.exp(before), (16, KEY_DIM)
        ).astype(BF)

    def state_copy(d, sender):
        return remote(
            state_out, state_in.at[sender], state_send.at[d - 1], state_recv.at[sender],
            {"sp": me + d},
        )

    for d in range(1, sp):
        @pl.when(me + d < sp)
        def _():
            state_copy(d, me).start()

    @pl.when(me >= 1)
    def _():
        edge.wait_recv()

    qi = lax.broadcasted_iota(jnp.int32, (WINDOW, 2 * WINDOW), 0)
    ki = lax.broadcasted_iota(jnp.int32, (WINDOW, 2 * WINDOW), 1)
    distance = qi + WINDOW - ki
    inside = (distance >= 0) & (distance < WINDOW)
    for b in range(fs):
        for w in range(rows // WINDOW):
            r0 = w * WINDOW
            here = proj[b, r0 : r0 + WINDOW, starts[4] : starts[4] + 2 * HEAD_DIM]
            if w == 0:
                past = edge_in[b]
                valid = inside & ((ki >= WINDOW) | (me >= 1))
            else:
                past = proj[b, r0 - WINDOW : r0, starts[4] : starts[4] + 2 * HEAD_DIM]
                valid = inside
            band = jnp.concatenate([past, here], 0)
            bk = band[:, :HEAD_DIM]
            bv = band[:, HEAD_DIM:]
            for h in range(heads):
                q0 = starts[1] + h * HEAD_DIM
                q = proj[b, r0 : r0 + WINDOW, q0 : q0 + HEAD_DIM]
                s = jnp.where(valid, nt(q, bk) * HEAD_DIM**-0.5, -1e30)
                sink = sinks[:, h : h + 1]
                top = jnp.maximum(jnp.max(s, -1, keepdims=True), sink)
                e = jnp.exp(s - top)
                den = jnp.sum(e, -1, keepdims=True) + jnp.exp(sink - top)
                a = nn((e / den).astype(BF), bv).astype(BF)
                h0 = VALUE_DIM + h * HEAD_DIM
                hidden[b, r0 : r0 + WINDOW, h0 : h0 + HEAD_DIM] = a

    for i in range(sp - 1):
        @pl.when(i < me)
        def _():
            state_copy(1, i).wait_recv()

        @pl.when(i >= me)
        def _():
            state_in[i] = jnp.zeros(state_in.shape[1:], BF)

    for b in range(fs):
        half = (b % 2) * KEY_DIM
        incoming = jnp.zeros((VALUE_DIM, KEY_DIM), F32)
        for i in range(sp - 1):
            got = state_in[i, b // 2, :VALUE_DIM, half : half + KEY_DIM].astype(F32)
            kept = state_in[i, b // 2, VALUE_DIM : VALUE_DIM + 1, half : half + KEY_DIM].astype(F32)
            incoming = jnp.where(i < me, kept * incoming + got, incoming)
        o = local_out[b] + nt(q_far[b], incoming.astype(BF))
        hidden[b, :, :VALUE_DIM] = rms_rows(o, hgain_ref[...]).astype(BF)

    forward = 2 * me < sp
    nc = o_buf.shape[2]

    def chunk(t):
        return lax.rem(jnp.where(forward, me + t, me - t) + sp, sp)

    def half_copy(s):
        return remote(half_out.at[s], half_in.at[s], half_send.at[s], half_recv.at[s], {"tp": 1 - c})

    def piece_copy(s, d, target):
        return remote(
            piece_out.at[s, d - 1], piece_in.at[s, d - 1],
            piece_send.at[s, d - 1], piece_recv.at[s, d - 1], {"fs": target},
        )

    def produce(t):
        s = chunk(t)

        @pl.when(jnp.logical_not(inner) & (t > 0))
        def _():
            o_copy(s, 0, False).wait_recv()

        w = o_buf[s]
        for b in range(fs):
            part = nn(hidden[b], w)
            lo, hi = part[:own], part[own:]
            half_out[s, b] = jnp.where(c == 0, hi, lo).astype(BF)
            half_own[s, b] = jnp.where(c == 0, lo, hi)
        half_copy(s).start()

    def combine(t):
        s = chunk(t)
        half_copy(s).wait_recv()
        for d in range(1, fs):
            to = lax.rem(f + d, fs)
            piece_out[s, d - 1] = (half_own[s, to] + half_in[s, to].astype(F32)).astype(BF)
            piece_copy(s, d, to).start()
        piece_own[s] = half_own[s, f] + half_in[s, f].astype(F32)

    def finish(t):
        s = chunk(t)
        total = piece_own[s]
        for d in range(1, fs):
            piece_copy(s, d, f).wait_recv()
            total += piece_in[s, d - 1].astype(F32)
        if len(out_ref.shape) == 2:
            out_ref[:, pl.ds(pl.multiple_of(s * nc, nc), nc)] = total.astype(BF)
        else:
            out_ref[s] = total.astype(BF)

    produce(0)

    def steady(t, _):
        produce(t)
        combine(t - 1)
        return 0

    lax.fori_loop(1, sp, steady, 0)
    combine(sp - 1)

    def close(t, _):
        finish(t)
        s = chunk(t)
        half_copy(s).wait_send()
        for d in range(1, fs):
            piece_copy(s, d, f).wait_send()
        return 0

    lax.fori_loop(0, sp, close, 0)

    for k in range(sp - 1):
        @pl.when((me - k >= 0) & (me + 1 < sp))
        def _():
            l_copy(me - k, 0, False).wait_send()
            w_copy(me - k, 0, False).wait_send()
            o_copy(me - k, 0, False).wait_send()

        @pl.when((me + k < sp) & (me >= 1))
        def _():
            l_copy(me + k, 1, False).wait_send()
            w_copy(me + k, 1, False).wait_send()
            o_copy(me + k, 1, False).wait_send()

    for i in range(sp):
        @pl.when(i != me)
        def _():
            for copy in pair_copies(i, side):
                copy.wait_send()

    for d in range(1, plane):
        tok_copy(d, mine, mine).wait_send()

    @pl.when(me + 1 < sp)
    def _():
        edge.wait_send()

    for d in range(1, sp):
        @pl.when(me + d < sp)
        def _():
            state_copy(d, me).wait_send()


def per_device(
    tokens,
    norm_gain,
    gla_query_weight,
    gla_key_weight,
    gla_value_weight,
    decay_down,
    decay_up,
    decay_bias,
    head_gain,
    window_query_weight,
    window_key_weight,
    window_value_weight,
    sink_logit,
    gla_output_weight,
    window_output_weight,
):
    fs, tp, sp = (lax.axis_size(n) for n in ("fs", "tp", "sp"))
    low = decay_down.T
    own = tokens.shape[1]
    rows = own * tp
    kc = decay_down.shape[0]
    width = VALUE_DIM + 4 * HEAD_DIM + 2 * KEY_DIM
    rank = low.shape[0]
    depth = (gla_output_weight.shape[0] + window_output_weight.shape[0]) // fs
    nc = gla_output_weight.shape[1]
    flat = nc % 128 == 0
    vm = pltpu.VMEM
    dma = pltpu.SemaphoreType.DMA
    scratch = [
        vm((fs * rows, tokens.shape[2]), BF),
        vm((sp * kc, width), BF),
        vm((sp, rank, kc), BF),
        vm((sp, depth, nc), BF),
        vm((fs, rows, width + 128), BF),
        vm((fs, WINDOW, 2 * HEAD_DIM), BF),
        vm((fs, WINDOW, 2 * HEAD_DIM), BF),
        vm((fs // 2, VALUE_DIM + 16, 2 * KEY_DIM), BF),
        vm((sp, fs // 2, VALUE_DIM + 16, 2 * KEY_DIM), BF),
        vm((fs, rows, VALUE_DIM), F32),
        vm((fs, rows, KEY_DIM), BF),
        vm((fs, rows, depth), BF),
        vm((sp, fs, own, nc), BF),
        vm((sp, fs, own, nc), BF),
        vm((sp, fs, own, nc), F32),
        vm((sp, fs - 1, own, nc), BF),
        vm((sp, fs - 1, own, nc), BF),
        vm((sp, own, nc), F32),
        dma((6,)),
        dma((fs * tp - 1,)),
        dma((fs * tp - 1,)),
        dma((2, sp)),
        dma((sp,)),
        dma((2, sp)),
        dma((sp,)),
        dma((2, sp)),
        dma((sp,)),
        dma((sp,)),
        dma((sp,)),
        dma((sp,)),
        dma((sp,)),
        dma((2, sp)),
        dma((sp,)),
        dma((2,)),
        dma((sp,)),
        dma((sp,)),
        dma((sp,)),
        dma((sp,)),
        dma((sp, fs - 1)),
        dma((sp, fs - 1)),
    ]
    spec = pl.BlockSpec(memory_space=pltpu.VMEM)
    anywhere = pl.BlockSpec(memory_space=pl.ANY)
    mixed = pl.pallas_call(
        functools.partial(mixer_kernel, (sp, fs, tp)),
        out_shape=jax.ShapeDtypeStruct((own, sp * nc) if flat else (sp, own, nc), BF),
        in_specs=[
            anywhere if i in (1, 2, 8, 9) else spec for i in range(15)
        ],
        out_specs=spec,
        scratch_shapes=scratch,
        compiler_params=pltpu.CompilerParams(
            has_side_effects=True, vmem_limit_bytes=60 * 1024 * 1024
        ),
    )(
        tokens[0],
        gla_value_weight,
        window_query_weight,
        gla_query_weight,
        gla_key_weight,
        window_key_weight,
        window_value_weight,
        low,
        gla_output_weight,
        window_output_weight,
        norm_gain[None],
        decay_up,
        decay_bias[None],
        head_gain[None],
        sink_logit[None],
    )
    return (mixed if flat else mixed.transpose(1, 0, 2)).reshape(1, own, sp * nc)


def solution(mesh):
    in_specs = (
        P("fs", ("sp", "tp"), None),
        P(),
        P("sp", "tp"),
        P("sp", "tp"),
        P("sp", "tp"),
        P("sp", None),
        P(None, "tp"),
        P("tp"),
        P(),
        P("sp", "tp"),
        P("sp", "tp"),
        P("sp", "tp"),
        P("tp"),
        P("tp", "sp"),
        P("tp", "sp"),
    )
    out_specs = P("fs", ("sp", "tp"), None)
    return jax.shard_map(
        per_device, mesh=mesh, in_specs=in_specs, out_specs=out_specs, check_vma=False
    )
```

profile of v0, /device:TPU:25, one launch (start us, length us, event | category | flops | bytes accessed | tf_op | source)
XLA Modules:
  0.0 88.2 jit_solution(6236679166635708858)
XLA Ops:
  0.0 86.5 %shard_map.145 = bf16[64,2048]{1,0:T(8,128)(2,1)} custom-call(bf16[64,2048]{1,0:T(8,128)(2,1)} %bitcast.8, bf16[512,512]{1,0:T(8,128)(2,1)} %gv_ref.1, bf16[512,512]{1,0:T(8,128)(2,1)} %wq_ref.1, bf16[512,256]{1,0:T(8,128)(2,1)} %gq_ref.1, bf16[512,256]{1,0:T(8,128)(2,1)} %gk_ref.1, bf16[512,128]{1,0:T(8,128)(2,1)} %wk_ref.1, bf16[512,128]{1,0:T(8,128)(2,1)} %wv_ref.1, ...), custom_call_target="tpu_custom_call" | custom-call | tf_op jit(solution)/shard_map/pallas_call | solution.py:595
  86.5 1.7 %copy.17 = bf16[1,64,2048]{2,1,0:T(8,128)(2,1)} copy(bf16[1,64,2048]{2,1,0:T(8,128)(2,1)} %bitcast.7) | data formatting | bytes 524288
where the time goes:
time: 88.4 us; the launch traced here: 88.2 us
  Pallas kernels  86.5 us (98%)
  local copies, waits for them, and re-layouts  1.67 us (2%)
    pallas_call x1, Pallas kernels, per_device(): pl.pallas_call(functools.partial(mixer_kernel, (sp, fs, tp)), out_shape=j...  86.5 us

commit v1 on v0

--- a/solution.py
+++ b/solution.py
@@ -519,6 +519,648 @@
             state_copy(d, me).wait_send()
 
 
+def roll_half(a):
+    return jnp.concatenate([a[:, a.shape[1] // 2 :], a[:, : a.shape[1] // 2]], 1)
+
+
+def fold_kernel(
+    sizes,
+    tok_ref,
+    gv_ref,
+    wq_ref,
+    gq_ref,
+    gk_ref,
+    wk_ref,
+    wv_ref,
+    low_ref,
+    go_ref,
+    wo_ref,
+    ngain_ref,
+    up_ref,
+    bias_ref,
+    hgain_ref,
+    sink_ref,
+    out_ref,
+    x_buf,
+    ww,
+    wg,
+    wl,
+    o_buf,
+    tiles,
+    qw,
+    kvb,
+    gvb,
+    qkb,
+    lowb,
+    decays,
+    totals,
+    states,
+    state_out,
+    state_in,
+    local_out,
+    q_far,
+    hidden,
+    half_out,
+    half_in,
+    half_own,
+    piece_out,
+    piece_in,
+    piece_own,
+    local_sem,
+    x_send,
+    x_recv,
+    w_send,
+    w_recv,
+    p_send,
+    p_recv,
+    o_send,
+    o_recv,
+    edge_sem,
+    state_sem,
+    hid_send,
+    hid_recv,
+    half_send,
+    half_recv,
+    piece_send,
+    piece_recv,
+):
+    sp, fs, tp = sizes
+    me = lax.axis_index("sp")
+    f = lax.axis_index("fs")
+    c = lax.axis_index("tp")
+    own = tok_ref.shape[0]
+    rows = own * tp
+    kc = gv_ref.shape[0]
+    part = kc // 2
+    lpart = low_ref.shape[0] // 2
+    MESH = pl.DeviceIdType.MESH
+    pair = 2 * KEY_DIM
+    wide = VALUE_DIM + pair
+
+    slot = lax.rem(me, 2)
+    far_slot = 1 - slot
+    inner = (me >= 1) & (me + 1 < sp)
+    outer = jnp.logical_not(inner)
+    middle = 1 + slot
+    outside = (sp - 1) * (me - 1)
+    buddy = me + 1 - 2 * slot
+    third = 2 - me // 2
+    fourth = third + 1 - 2 * lax.rem(third, 2)
+    chunks = [me, buddy, third, fourth]
+    side = lax.rem(f, 2)
+    xn = f + 1 - 2 * side
+    yn = lax.rem(f + 2, fs)
+    n1 = xn * (1 - c) + yn * c
+    n2 = xn * c + yn * (1 - c)
+
+    def remote(src, dst, ssem, rsem, target):
+        return pltpu.make_async_remote_copy(
+            src_ref=src, dst_ref=dst, send_sem=ssem, recv_sem=rsem,
+            device_id=target, device_id_type=MESH,
+        )
+
+    barrier = pltpu.get_barrier_semaphore()
+
+    def greet(target):
+        pl.semaphore_signal(barrier, inc=1, device_id=target, device_id_type=MESH)
+
+    greet({"tp": 1 - c})
+    for d in range(1, fs):
+        greet({"fs": lax.rem(f + d, fs)})
+
+    @pl.when(me + 1 < sp)
+    def _():
+        greet({"sp": me + 1})
+
+    @pl.when(me >= 1)
+    def _():
+        greet({"sp": me - 1})
+
+    def lanes(ref, at, width):
+        return ref.at[:, pl.ds(pl.multiple_of(at * width, width), width)]
+
+    def depth(ref, width):
+        return ref.at[pl.ds(pl.multiple_of(f * width, width), width)]
+
+    def slice_rows(ref, s):
+        return ref.at[pl.ds(pl.multiple_of(s * kc, kc), kc)]
+
+    gd = go_ref.shape[0] // fs
+    wd = wo_ref.shape[0] // fs
+    heads = sink_ref.shape[1] // fs
+    wq_cols = heads * HEAD_DIM
+    kv = (f * heads) // (SWA_HEADS // KV_HEADS)
+    copies_in = [
+        (lanes(gq_ref, f // 2, pair), tiles.at[0]),
+        (lanes(gk_ref, f // 2, pair), tiles.at[1]),
+        (wk_ref, tiles.at[2]),
+        (wv_ref, tiles.at[3]),
+        (lanes(wq_ref, f, wq_cols), slice_rows(ww, me).at[:, :wq_cols]),
+        (lanes(gv_ref, f, VALUE_DIM), slice_rows(wg, me).at[:, :VALUE_DIM]),
+        (low_ref, wl.at[me]),
+        (depth(go_ref, gd), o_buf.at[me, pl.ds(0, gd)]),
+        (depth(wo_ref, wd), o_buf.at[me, pl.ds(gd, wd)]),
+    ]
+    locals_ = [
+        pltpu.make_async_copy(a, b, local_sem.at[i]) for i, (a, b) in enumerate(copies_in)
+    ]
+    for copy in locals_:
+        copy.start()
+
+    def block(s, i):
+        return x_buf.at[s, pl.ds(pl.multiple_of(i * own, own), own)]
+
+    mine = f * tp + c
+    b1, b2, b3 = n1 * tp + c, n2 * tp + c, (fs - 1 - f) * tp + c
+
+    normed = rms_rows(tok_ref[...].astype(F32), ngain_ref[...]).astype(BF)
+    x_buf[slot, pl.ds(pl.multiple_of(mine * own, own), own)] = normed
+
+    def x_copy(s, i, k, target):
+        return remote(block(s, i), block(s, i), x_send.at[s, k], x_recv.at[s, i], target)
+
+    SIB = {"tp": 1 - c}
+
+    def x_first(s):
+        return [
+            x_copy(s, mine, 0, {"fs": n1}),
+            x_copy(s, mine, 1, {"fs": n2}),
+            x_copy(s, mine, 2, SIB),
+        ]
+
+    def x_from1(s):
+        return [x_copy(s, b1, 3, {"fs": n2}), x_copy(s, b1, 4, SIB)]
+
+    def x_from2(s):
+        return [x_copy(s, b2, 5, SIB)]
+
+    def x_from3(s):
+        return [x_copy(s, b3, 6, SIB)]
+
+    def x_all(s):
+        return x_first(s) + x_from1(s) + x_from2(s) + x_from3(s)
+
+    def x_out():
+        return x_copy(slot, mine, 0, {"sp": middle})
+
+    def kv_rows(s, h):
+        at = pl.multiple_of(s * kc + h * part, part)
+        return ww.at[pl.ds(at, part), wq_cols:]
+
+    def low_rows(s, h):
+        return wl.at[s, pl.ds(pl.multiple_of(h * lpart, lpart), lpart)]
+
+    def w_copy(kind, s):
+        ref = (
+            lambda: slice_rows(ww, s).at[:, :wq_cols],
+            lambda: kv_rows(s, side),
+            lambda: low_rows(s, c),
+            lambda: slice_rows(wg, s),
+        )[kind]()
+        return remote(ref, ref, w_send.at[kind, s], w_recv.at[kind, s], {"sp": middle})
+
+    def kv_share(s, h):
+        return remote(
+            kv_rows(s, h), kv_rows(s, h), p_send.at[0, s], p_recv.at[0, s], {"fs": xn}
+        )
+
+    def low_share(s, h):
+        return remote(low_rows(s, h), low_rows(s, h), p_send.at[1, s], p_recv.at[1, s], SIB)
+
+    def o_copy(way, s):
+        target = {"sp": middle if way == 0 else outside}
+        return remote(o_buf.at[s], o_buf.at[s], o_send.at[way, s], o_recv.at[s], target)
+
+    def start(copies):
+        for copy in copies:
+            copy.start()
+
+    pl.semaphore_wait(barrier, fs + jnp.where(inner, 2, 1))
+
+    @pl.when(outer)
+    def _():
+        x_out().start()
+
+    @pl.when(inner)
+    def _():
+        start(x_first(slot))
+
+    for copy in locals_[:7]:
+        copy.wait()
+    own_rows = pl.ds(pl.multiple_of(me * kc, kc), kc)
+
+    def half_of(i, width, which):
+        return jnp.where(which == 0, tiles[i, :, :width], tiles[i, :, width:])
+
+    ww[own_rows, wq_cols:] = jnp.concatenate(
+        [half_of(2, HEAD_DIM, kv), half_of(3, HEAD_DIM, kv)], 1
+    )
+    for kind in range(3):
+        w_copy(kind, me).start()
+    wg[own_rows, VALUE_DIM:] = jnp.concatenate(
+        [half_of(0, KEY_DIM, side), half_of(1, KEY_DIM, side)], 1
+    )
+    w_copy(3, me).start()
+    for copy in locals_[7:]:
+        copy.wait()
+
+    @pl.when(outer)
+    def _():
+        o_copy(0, me).start()
+
+    lane = lax.broadcasted_iota(jnp.int32, (rows, pair), 1)
+    row = lax.broadcasted_iota(jnp.int32, (rows, pair), 0)
+    left = lane < KEY_DIM
+    early = row < SPAN
+    same = (row < SPAN) == (lane < SPAN)
+    diagonal = same & (row >= lane)
+    below = (row >= SPAN) & (lane < SPAN)
+
+    edge = remote(kvb.at[2], kvb.at[0], edge_sem.at[0], edge_sem.at[1], {"sp": me + 1})
+    state = remote(state_out, state_in, state_sem.at[0], state_sem.at[1], {"sp": me + 1})
+
+    def hid_part(s, i):
+        return hidden.at[s, :, i * VALUE_DIM : (i + 1) * VALUE_DIM]
+
+    def hid_copy(i, s):
+        return remote(
+            hid_part(s, i), hid_part(s, i), hid_send.at[i], hid_recv.at[i], {"sp": outside}
+        )
+
+    def seq(b):
+        if isinstance(b, int):
+            return pl.ds(b * rows, rows)
+        return pl.ds(pl.multiple_of(b * rows, rows), rows)
+
+    @pl.when(inner)
+    def _():
+        o_copy(1, me).start()
+        x_copy(far_slot, mine, 0, SIB).wait_recv()
+        start(x_first(far_slot))
+
+        def got_first(s, onward):
+            for kind in range(3):
+                w_copy(kind, s).wait_recv()
+                if onward:
+                    w_copy(kind, s).start()
+            kv_share(s, side).start()
+            low_share(s, c).start()
+
+        def neighbours(s):
+            x_copy(s, b1, 0, SIB).wait_recv()
+            start(x_from1(s))
+            x_copy(s, b2, 0, SIB).wait_recv()
+            start(x_from2(s))
+
+        def corner(s):
+            x_copy(s, b3, 0, SIB).wait_recv()
+            start(x_from3(s))
+
+        got_first(third, False)
+        neighbours(slot)
+        corner(slot)
+        got_first(buddy, True)
+        neighbours(far_slot)
+        w_copy(3, buddy).wait_recv()
+        w_copy(3, buddy).start()
+        o_copy(0, me).start()
+        corner(far_slot)
+        got_first(fourth, False)
+        for s in chunks[1:]:
+            kv_share(s, 1 - side).wait_recv()
+            low_share(s, 1 - c).wait_recv()
+        for s in range(2):
+            for g in range(fs):
+                x_copy(s, g * tp + 1 - c, 0, SIB).wait_recv()
+
+        def first_maps(i, _):
+            s = i // fs
+            b = lax.rem(i, fs)
+            x = x_buf[s, seq(b)]
+            p = nn(x, ww[...])
+            qw[s, seq(b)] = (p[:, :wq_cols].astype(BF).astype(F32) * HEAD_DIM**-0.5).astype(BF)
+            kvb[s + 1, seq(b)] = p[:, wq_cols:].astype(BF)
+            low = nt(x[:, :kc], wl[0])
+            for j in range(1, sp):
+                low += nt(x[:, j * kc : (j + 1) * kc], wl[j])
+            lowb[s, seq(b)] = low.astype(BF)
+            return 0
+
+        lax.fori_loop(0, 2 * fs, first_maps, 0)
+
+        @pl.when(me == 1)
+        def _():
+            edge.start()
+            kvb[0] = jnp.zeros(kvb.shape[1:], BF)
+            state_in[...] = jnp.zeros_like(state_in)
+
+        up = jnp.where(side == 0, up_ref[:, :KEY_DIM], up_ref[:, KEY_DIM:pair])
+        up1 = jnp.where(side == 0, up_ref[:, pair : pair + KEY_DIM], up_ref[:, pair + KEY_DIM :])
+        up = jnp.where(f // 2 == 0, up, up1)
+        bs = [bias_ref[:, i * KEY_DIM : (i + 1) * KEY_DIM] for i in range(fs)]
+        bias = bs[0]
+        for i in range(1, fs):
+            bias = jnp.where(f == i, bs[i], bias)
+        up_l = jnp.concatenate([up, jnp.zeros_like(up)], 1)
+        up_r = jnp.concatenate([jnp.zeros_like(up), up], 1)
+        bias2 = jnp.concatenate([bias, bias], 1)
+        tri = diagonal.astype(F32)
+        for s in range(2):
+            for p in range(fs // 2):
+                z = nn(lowb[s, seq(2 * p)], up_l) + nn(lowb[s, seq(2 * p + 1)], up_r) + bias2
+                rate = (jnp.minimum(z, 0.0) - jnp.log1p(jnp.exp(-jnp.abs(z)))) / SOFTMAX_TEMPER
+                within = exact(tri, rate)
+                t0, t1 = within[SPAN - 1 : SPAN], within[rows - 1 :]
+                grow = jnp.exp(within) * KEY_DIM**-0.5
+                end = jnp.exp(jnp.where(early, t0, t1) - within)
+                decays[s, p, 0] = grow
+                decays[s, p, 1] = jnp.exp(-within)
+                decays[s, p, 2] = end
+                decays[s, p, 3] = grow * jnp.where(early, 1.0, jnp.exp(t0))
+                decays[s, p, 4] = end * jnp.where(early, jnp.exp(t1), 1.0)
+                totals[s, p] = jnp.broadcast_to(jnp.exp(t0 + t1), totals.shape[2:])
+
+        qi = lax.broadcasted_iota(jnp.int32, (WINDOW, 2 * WINDOW), 0)
+        ki = lax.broadcasted_iota(jnp.int32, (WINDOW, 2 * WINDOW), 1)
+        distance = qi + WINDOW - ki
+        inside = (distance >= 0) & (distance < WINDOW)
+        sinks = sink_ref[:, :heads]
+        for i in range(1, fs):
+            sinks = jnp.where(f == i, sink_ref[:, i * heads : (i + 1) * heads], sinks)
+
+        def window(s):
+            valid = inside & ((ki >= WINDOW) | (me > 1) | (s > 0))
+
+            def one(b, _):
+                band = jnp.concatenate([kvb[s, seq(b)], kvb[s + 1, seq(b)]], 0)
+                q = qw[s, seq(b)].astype(F32)
+                outs = []
+                for h in range(heads):
+                    qh = jnp.where(left, q if h == 0 else roll_half(q), 0.0).astype(BF)
+                    sc = jnp.where(valid, nt(qh, band), -1e30)
+                    sink = sinks[:, h : h + 1]
+                    top = jnp.maximum(jnp.max(sc, -1, keepdims=True), sink)
+                    e = jnp.exp(sc - top)
+                    den = jnp.sum(e, -1, keepdims=True) + jnp.exp(sink - top)
+                    outs.append(nn((e * (1.0 / den)).astype(BF), band))
+                hidden[s, seq(b), VALUE_DIM:] = jnp.where(left, roll_half(outs[0]), outs[1]).astype(BF)
+                return 0
+
+            for b in range(fs):
+                one(b, 0)
+
+        window(far_slot)
+        hid_copy(1, far_slot).start()
+        w_copy(3, third).wait_recv()
+        w_copy(3, fourth).wait_recv()
+
+        def second_maps(i, _):
+            s = i // fs
+            b = lax.rem(i, fs)
+            p = nn(x_buf[s, seq(b)], wg[...]).astype(BF)
+            gvb[s, seq(b)] = p[:, :VALUE_DIM]
+            qkb[s, seq(b)] = p[:, VALUE_DIM:].astype(F32)
+            return 0
+
+        lax.fori_loop(0, 2 * fs, second_maps, 0)
+
+        def keys(s, p):
+            return jnp.where(left, roll_half(qkb[s, seq(2 * p)]), qkb[s, seq(2 * p + 1)])
+
+        def queries(s, p):
+            return jnp.where(left, qkb[s, seq(2 * p)], roll_half(qkb[s, seq(2 * p + 1)]))
+
+        for s in range(2):
+            for p in range(fs // 2):
+                k_far = (keys(s, p) * decays[s, p, 4]).astype(BF)
+                states[s, p] = jnp.where(
+                    left, tn(gvb[s, seq(2 * p)], k_far), tn(gvb[s, seq(2 * p + 1)], k_far)
+                )
+        for p in range(fs // 2):
+            state_out[p] = (totals[1, p, :1] * states[0, p] + states[1, p]).astype(BF)
+
+        @pl.when(me == 1)
+        def _():
+            state.start()
+
+        o_copy(0, buddy).wait_recv()
+        o_copy(0, buddy).start()
+
+        for s in range(2):
+            for p in range(fs // 2):
+                k = keys(s, p)
+                q = queries(s, p)
+                qd = q * decays[s, p, 0]
+                qf = q * decays[s, p, 3]
+                kd = (k * decays[s, p, 1]).astype(BF)
+                ke = (k * decays[s, p, 2]).astype(BF)
+                for j in range(2):
+                    here = left if j == 0 else jnp.logical_not(left)
+                    qj = jnp.where(here, qd, 0.0).astype(BF)
+                    scores = jnp.where(
+                        diagonal, nt(qj, kd), jnp.where(below, nt(qj, ke), 0.0)
+                    ).astype(BF)
+                    local_out[s, seq(2 * p + j)] = nn(scores, gvb[s, seq(2 * p + j)])
+                    q_far[s, seq(2 * p + j)] = jnp.where(here, qf, 0.0).astype(BF)
+
+        @pl.when(me > 1)
+        def _():
+            state.wait_recv()
+
+        def finish_state(s):
+            for p in range(fs // 2):
+                arrived = state_in[p].astype(F32)
+                entering = jnp.where(s == 0, arrived, totals[0, p, :1] * arrived + states[0, p])
+                entering = entering.astype(BF)
+                for j in range(2):
+                    b = 2 * p + j
+                    o = local_out[s, seq(b)] + nt(q_far[s, seq(b)], entering)
+                    hidden[s, seq(b), :VALUE_DIM] = rms_rows(o, hgain_ref[...]).astype(BF)
+
+        finish_state(far_slot)
+        hid_copy(0, far_slot).start()
+        finish_state(slot)
+
+        @pl.when(me > 1)
+        def _():
+            edge.wait_recv()
+
+        window(slot)
+
+    @pl.when(outer)
+    def _():
+        hid_copy(1, slot).wait_recv()
+        hid_copy(0, slot).wait_recv()
+
+    nc = o_buf.shape[2]
+
+    def half_copy(s):
+        return remote(half_out.at[s], half_in.at[s], half_send.at[s], half_recv.at[s], SIB)
+
+    def piece_copy(s, d, target):
+        return remote(
+            piece_out.at[s, d - 1], piece_in.at[s, d - 1],
+            piece_send.at[s, d - 1], piece_recv.at[s, d - 1], {"fs": target},
+        )
+
+    def produce(t):
+        s = chunks[t]
+        if t == 1:
+            @pl.when(outer)
+            def _():
+                o_copy(0, s).wait_recv()
+        if t > 1:
+            o_copy(0, s).wait_recv()
+
+            @pl.when(inner)
+            def _():
+                o_copy(1, s).start()
+
+        w = o_buf[s]
+        for b in range(fs):
+            partial = nn(hidden[slot, seq(b)], w)
+            lo, hi = partial[:own], partial[own:]
+            half_out[s, b] = jnp.where(c == 0, hi, lo).astype(BF)
+            half_own[s, b] = jnp.where(c == 0, lo, hi)
+        half_copy(s).start()
+
+    def combine(t):
+        s = chunks[t]
+        half_copy(s).wait_recv()
+        for d in range(1, fs):
+            to = lax.rem(f + d, fs)
+            piece_out[s, d - 1] = (half_own[s, to] + half_in[s, to].astype(F32)).astype(BF)
+            piece_copy(s, d, to).start()
+        piece_own[s] = half_own[s, f] + half_in[s, f].astype(F32)
+
+    def finish(t):
+        s = chunks[t]
+        total = piece_own[s]
+        for d in range(1, fs):
+            piece_copy(s, d, f).wait_recv()
+            total += piece_in[s, d - 1].astype(F32)
+        out_ref[:, pl.ds(pl.multiple_of(s * nc, nc), nc)] = total.astype(BF)
+
+    produce(0)
+    for t in range(1, sp):
+        produce(t)
+        combine(t - 1)
+    combine(sp - 1)
+    for t in range(sp):
+        finish(t)
+    for t in range(sp):
+        s = chunks[t]
+        half_copy(s).wait_send()
+        for d in range(1, fs):
+            piece_copy(s, d, f).wait_send()
+
+    for kind in range(4):
+        w_copy(kind, me).wait_send()
+    o_copy(0, me).wait_send()
+
+    @pl.when(outer)
+    def _():
+        x_out().wait_send()
+
+    @pl.when(inner)
+    def _():
+        for s in range(2):
+            for copy in x_all(s):
+                copy.wait_send()
+        for kind in range(4):
+            w_copy(kind, buddy).wait_send()
+        for s in chunks[1:]:
+            kv_share(s, side).wait_send()
+            low_share(s, c).wait_send()
+        o_copy(0, buddy).wait_send()
+        for s in (me, third, fourth):
+            o_copy(1, s).wait_send()
+        for i in range(2):
+            hid_copy(i, far_slot).wait_send()
+
+        @pl.when(me == 1)
+        def _():
+            edge.wait_send()
+            state.wait_send()
+
+
+def fold_call(sizes, operands):
+    sp, fs, tp = sizes
+    own, d = operands[0].shape
+    rows = own * tp
+    kc = operands[1].shape[0]
+    rank = operands[7].shape[0]
+    depth = (operands[8].shape[0] + operands[9].shape[0]) // fs
+    nc = operands[8].shape[1]
+    pair = 2 * KEY_DIM
+    all_rows = fs * rows
+    pairs = fs // 2
+    vm = pltpu.VMEM
+    dma = pltpu.SemaphoreType.DMA
+    scratch = [
+        vm((2, all_rows, d), BF),
+        vm((d, 2 * pair), BF),
+        vm((d, VALUE_DIM + pair), BF),
+        vm((sp, rank, kc), BF),
+        vm((sp, depth, nc), BF),
+        vm((4, kc, pair), BF),
+        vm((2, all_rows, pair), BF),
+        vm((3, all_rows, pair), BF),
+        vm((2, all_rows, VALUE_DIM), BF),
+        vm((2, all_rows, pair), F32),
+        vm((2, all_rows, rank), BF),
+        vm((2, pairs, 5, rows, pair), F32),
+        vm((2, pairs, 8, pair), F32),
+        vm((2, pairs, VALUE_DIM, pair), F32),
+        vm((pairs, VALUE_DIM, pair), BF),
+        vm((pairs, VALUE_DIM, pair), BF),
+        vm((2, all_rows, VALUE_DIM), F32),
+        vm((2, all_rows, pair), BF),
+        vm((2, all_rows, depth), BF),
+        vm((sp, fs, own, nc), BF),
+        vm((sp, fs, own, nc), BF),
+        vm((sp, fs, own, nc), F32),
+        vm((sp, fs - 1, own, nc), BF),
+        vm((sp, fs - 1, own, nc), BF),
+        vm((sp, own, nc), F32),
+        dma((9,)),
+        dma((2, 7)),
+        dma((2, fs * tp)),
+        dma((4, sp)),
+        dma((4, sp)),
+        dma((2, sp)),
+        dma((2, sp)),
+        dma((2, sp)),
+        dma((sp,)),
+        dma((2,)),
+        dma((2,)),
+        dma((2,)),
+        dma((2,)),
+        dma((sp,)),
+        dma((sp,)),
+        dma((sp, fs - 1)),
+        dma((sp, fs - 1)),
+    ]
+    spec = pl.BlockSpec(memory_space=pltpu.VMEM)
+    anywhere = pl.BlockSpec(memory_space=pl.ANY)
+    return pl.pallas_call(
+        functools.partial(fold_kernel, sizes),
+        out_shape=jax.ShapeDtypeStruct((own, sp * nc), BF),
+        in_specs=[anywhere if i in (1, 2, 3, 4, 5, 6, 8, 9) else spec for i in range(15)],
+        out_specs=spec,
+        scratch_shapes=scratch,
+        compiler_params=pltpu.CompilerParams(
+            has_side_effects=True, vmem_limit_bytes=60 * 1024 * 1024, collective_id=0
+        ),
+    )(*operands)
+
+
+def folds(sp, fs, tp, shape, rows, kc, width, rank, nc, depth):
+    whole_rows = rows == WINDOW == 2 * SPAN
+    lanes_fit = nc % 128 == 0 and kc % 128 == 0 and depth == 2 * VALUE_DIM
+    return sp == 4 and fs == 4 and tp == 2 and whole_rows and lanes_fit and rank % 32 == 0
+
+
 def per_device(
     tokens,
     norm_gain,
@@ -546,6 +1188,25 @@
     depth = (gla_output_weight.shape[0] + window_output_weight.shape[0]) // fs
     nc = gla_output_weight.shape[1]
     flat = nc % 128 == 0
+    operands = (
+        tokens[0],
+        gla_value_weight,
+        window_query_weight,
+        gla_query_weight,
+        gla_key_weight,
+        window_key_weight,
+        window_value_weight,
+        low,
+        gla_output_weight,
+        window_output_weight,
+        norm_gain[None],
+        decay_up,
+        decay_bias[None],
+        head_gain[None],
+        sink_logit[None],
+    )
+    if folds(sp, fs, tp, tokens.shape, rows, kc, width, rank, nc, depth):
+        return fold_call((sp, fs, tp), operands).reshape(1, own, sp * nc)
     vm = pltpu.VMEM
     dma = pltpu.SemaphoreType.DMA
     scratch = [
@@ -603,23 +1264,7 @@
         compiler_params=pltpu.CompilerParams(
             has_side_effects=True, vmem_limit_bytes=60 * 1024 * 1024
         ),
-    )(
-        tokens[0],
-        gla_value_weight,
-        window_query_weight,
-        gla_query_weight,
-        gla_key_weight,
-        window_key_weight,
-        window_value_weight,
-        low,
-        gla_output_weight,
-        window_output_weight,
-        norm_gain[None],
-        decay_up,
-        decay_bias[None],
-        head_gain[None],
-        sink_logit[None],
-    )
+    )(*operands)
     return (mixed if flat else mixed.transpose(1, 0, 2)).reshape(1, own, sp * nc)
 
 

time: 88.4 us -> 73.1 us (0.83)
  the two profiles are of different devices: /device:TPU:25 before, /device:TPU:0 now
where the time goes in v1:
time: 73.1 us; the launch traced here: 72.9 us
  Pallas kernels  71.3 us (98%)
  local copies, waits for them, and re-layouts  1.67 us (2%)
    pallas_call x1, Pallas kernels, fold_call(): pl.pallas_call(functools.partial(fold_kernel, sizes), out_shape=jax.Shape...  71.3 us
    unnamed x1, local copies, waits for them, and re-layouts  1.67 us

profile of v1, /device:TPU:0, one launch (start us, length us, event | category | flops | bytes accessed | tf_op | source)
XLA Modules:
  0.0 72.9 jit_solution(8973827194361178489)
XLA Ops:
  0.0 71.3 %shard_map.145 = bf16[64,2048]{1,0:T(8,128)(2,1)} custom-call(bf16[64,2048]{1,0:T(8,128)(2,1)} %bitcast.8, bf16[512,512]{1,0:T(8,128)(2,1)} %gv_ref.1, bf16[512,512]{1,0:T(8,128)(2,1)} %wq_ref.1, bf16[512,256]{1,0:T(8,128)(2,1)} %gq_ref.1, bf16[512,256]{1,0:T(8,128)(2,1)} %gk_ref.1, bf16[512,128]{1,0:T(8,128)(2,1)} %wk_ref.1, bf16[512,128]{1,0:T(8,128)(2,1)} %wv_ref.1, ...), custom_call_target="tpu_custom_call" | custom-call | tf_op jit(solution)/shard_map/pallas_call | solution.py:1146
  71.3 1.7 %copy.17 = bf16[1,64,2048]{2,1,0:T(8,128)(2,1)} copy(bf16[1,64,2048]{2,1,0:T(8,128)(2,1)} %bitcast.7) | data formatting | bytes 524288

commit v2 on v1

--- a/solution.py
+++ b/solution.py
@@ -525,7 +525,7 @@
 
 def fold_kernel(
     sizes,
-    tok_ref,
+    tok_in,
     gv_ref,
     wq_ref,
     gq_ref,
@@ -535,6 +535,13 @@
     low_ref,
     go_ref,
     wo_ref,
+    ngain_in,
+    up_in,
+    bias_in,
+    hgain_in,
+    sink_in,
+    out_hbm,
+    tok_ref,
     ngain_ref,
     up_ref,
     bias_ref,
@@ -551,7 +558,8 @@
     kvb,
     gvb,
     qkb,
-    lowb,
+    acc,
+    lowx,
     decays,
     totals,
     states,
@@ -567,6 +575,9 @@
     piece_in,
     piece_own,
     local_sem,
+    out_sem,
+    l_send,
+    l_recv,
     x_send,
     x_recv,
     w_send,
@@ -588,7 +599,7 @@
     me = lax.axis_index("sp")
     f = lax.axis_index("fs")
     c = lax.axis_index("tp")
-    own = tok_ref.shape[0]
+    own = tok_in.shape[0]
     rows = own * tp
     kc = gv_ref.shape[0]
     part = kc // 2
@@ -647,7 +658,7 @@
 
     gd = go_ref.shape[0] // fs
     wd = wo_ref.shape[0] // fs
-    heads = sink_ref.shape[1] // fs
+    heads = sink_in.shape[1] // fs
     wq_cols = heads * HEAD_DIM
     kv = (f * heads) // (SWA_HEADS // KV_HEADS)
     copies_in = [
@@ -658,13 +669,26 @@
         (lanes(wq_ref, f, wq_cols), slice_rows(ww, me).at[:, :wq_cols]),
         (lanes(gv_ref, f, VALUE_DIM), slice_rows(wg, me).at[:, :VALUE_DIM]),
         (low_ref, wl.at[me]),
-        (depth(go_ref, gd), o_buf.at[me, pl.ds(0, gd)]),
-        (depth(wo_ref, wd), o_buf.at[me, pl.ds(gd, wd)]),
+    ]
+    nc = o_buf.shape[3]
+    for h in range(2):
+        cut = pl.ds(h * nc, nc)
+        copies_in += [
+            (depth(go_ref, gd).at[:, cut], o_buf.at[me, h, pl.ds(0, gd)]),
+            (depth(wo_ref, wd).at[:, cut], o_buf.at[me, h, pl.ds(gd, wd)]),
+        ]
+    copies_in += [
+        (ngain_in, ngain_ref),
+        (tok_in, tok_ref),
+        (up_in, up_ref),
+        (bias_in, bias_ref),
+        (hgain_in, hgain_ref),
+        (sink_in, sink_ref),
     ]
     locals_ = [
         pltpu.make_async_copy(a, b, local_sem.at[i]) for i, (a, b) in enumerate(copies_in)
     ]
-    for copy in locals_:
+    for copy in locals_[11:] + locals_[:11]:
         copy.start()
 
     def block(s, i):
@@ -673,6 +697,8 @@
     mine = f * tp + c
     b1, b2, b3 = n1 * tp + c, n2 * tp + c, (fs - 1 - f) * tp + c
 
+    for copy in locals_[11:]:
+        copy.wait()
     normed = rms_rows(tok_ref[...].astype(F32), ngain_ref[...]).astype(BF)
     x_buf[slot, pl.ds(pl.multiple_of(mine * own, own), own)] = normed
 
@@ -727,9 +753,21 @@
     def low_share(s, h):
         return remote(low_rows(s, h), low_rows(s, h), p_send.at[1, s], p_recv.at[1, s], SIB)
 
-    def o_copy(way, s):
+    def o_copy(way, s, h):
         target = {"sp": middle if way == 0 else outside}
-        return remote(o_buf.at[s], o_buf.at[s], o_send.at[way, s], o_recv.at[s], target)
+        return remote(
+            o_buf.at[s, h], o_buf.at[s, h], o_send.at[way, s, h], o_recv.at[s, h], target
+        )
+
+    def l_copy(i, k, target):
+        return remote(lowx.at[i], lowx.at[i], l_send.at[k], l_recv.at[i], target)
+
+    def l_first():
+        peers = [{"fs": n1}, {"fs": n2}, {"fs": fs - 1 - f}, SIB]
+        return [l_copy(mine, k, peer) for k, peer in enumerate(peers)]
+
+    def l_onward():
+        return [l_copy(i, 4 + k, SIB) for k, i in enumerate((b1, b2, b3))]
 
     def start(copies):
         for copy in copies:
@@ -737,6 +775,10 @@
 
     pl.semaphore_wait(barrier, fs + jnp.where(inner, 2, 1))
 
+    LOW, KV, QUERY, STATE = 2, 1, 0, 3
+    locals_[6].wait()
+    w_copy(LOW, me).start()
+
     @pl.when(outer)
     def _():
         x_out().start()
@@ -745,7 +787,7 @@
     def _():
         start(x_first(slot))
 
-    for copy in locals_[:7]:
+    for copy in locals_[:6]:
         copy.wait()
     own_rows = pl.ds(pl.multiple_of(me * kc, kc), kc)
 
@@ -755,18 +797,19 @@
     ww[own_rows, wq_cols:] = jnp.concatenate(
         [half_of(2, HEAD_DIM, kv), half_of(3, HEAD_DIM, kv)], 1
     )
-    for kind in range(3):
-        w_copy(kind, me).start()
+    w_copy(KV, me).start()
+    w_copy(QUERY, me).start()
     wg[own_rows, VALUE_DIM:] = jnp.concatenate(
         [half_of(0, KEY_DIM, side), half_of(1, KEY_DIM, side)], 1
     )
-    w_copy(3, me).start()
-    for copy in locals_[7:]:
+    for copy in locals_[7:11]:
         copy.wait()
 
     @pl.when(outer)
     def _():
-        o_copy(0, me).start()
+        w_copy(STATE, me).start()
+        for h in range(2):
+            o_copy(0, me, h).start()
 
     lane = lax.broadcasted_iota(jnp.int32, (rows, pair), 1)
     row = lax.broadcasted_iota(jnp.int32, (rows, pair), 0)
@@ -794,17 +837,17 @@
 
     @pl.when(inner)
     def _():
-        o_copy(1, me).start()
-        x_copy(far_slot, mine, 0, SIB).wait_recv()
-        start(x_first(far_slot))
-
-        def got_first(s, onward):
-            for kind in range(3):
-                w_copy(kind, s).wait_recv()
-                if onward:
-                    w_copy(kind, s).start()
-            kv_share(s, side).start()
-            low_share(s, c).start()
+        for h in range(2):
+            o_copy(1, me, h).start()
+
+        def arrive(kind, s, onward):
+            w_copy(kind, s).wait_recv()
+            if onward:
+                w_copy(kind, s).start()
+            if kind == LOW:
+                low_share(s, c).start()
+            if kind == KV:
+                kv_share(s, side).start()
 
         def neighbours(s):
             x_copy(s, b1, 0, SIB).wait_recv()
@@ -816,37 +859,108 @@
             x_copy(s, b3, 0, SIB).wait_recv()
             start(x_from3(s))
 
-        got_first(third, False)
-        neighbours(slot)
-        corner(slot)
-        got_first(buddy, True)
-        neighbours(far_slot)
-        w_copy(3, buddy).wait_recv()
-        w_copy(3, buddy).start()
-        o_copy(0, me).start()
-        corner(far_slot)
-        got_first(fourth, False)
-        for s in chunks[1:]:
-            kv_share(s, 1 - side).wait_recv()
-            low_share(s, 1 - c).wait_recv()
-        for s in range(2):
+        def siblings(s):
             for g in range(fs):
                 x_copy(s, g * tp + 1 - c, 0, SIB).wait_recv()
 
-        def first_maps(i, _):
-            s = i // fs
-            b = lax.rem(i, fs)
-            x = x_buf[s, seq(b)]
-            p = nn(x, ww[...])
-            qw[s, seq(b)] = (p[:, :wq_cols].astype(BF).astype(F32) * HEAD_DIM**-0.5).astype(BF)
-            kvb[s + 1, seq(b)] = p[:, wq_cols:].astype(BF)
-            low = nt(x[:, :kc], wl[0])
+        def columns(s):
+            return pl.ds(pl.multiple_of(s * kc, kc), kc)
+
+        bs = [bias_ref[:, i * KEY_DIM : (i + 1) * KEY_DIM] for i in range(fs)]
+        ups = [up_ref[:, i * KEY_DIM : (i + 1) * KEY_DIM] for i in range(fs)]
+        bias, up = bs[0], ups[0]
+        for i in range(1, fs):
+            bias = jnp.where(f == i, bs[i], bias)
+            up = jnp.where(f == i, ups[i], up)
+        up_l = jnp.concatenate([up, jnp.zeros_like(up)], 1)
+        up_r = jnp.concatenate([jnp.zeros_like(up), up], 1)
+        bias2 = jnp.concatenate([bias, bias], 1)
+
+        def own_low():
+            at = pl.ds(pl.multiple_of(mine * own, own), own)
+            x = jnp.concatenate([x_buf[slot, at], x_buf[far_slot, at]], 0)
+            low = nt(wl[0], x[:, :kc])
             for j in range(1, sp):
-                low += nt(x[:, j * kc : (j + 1) * kc], wl[j])
-            lowb[s, seq(b)] = low.astype(BF)
-            return 0
-
-        lax.fori_loop(0, 2 * fs, first_maps, 0)
+                low += nt(wl[j], x[:, j * kc : (j + 1) * kc])
+            lowx[mine] = low.astype(BF)
+
+        def gate(p):
+            pre = []
+            for i in range(tp):
+                z = tn(lowx[2 * p * tp + i], up_l) + tn(lowx[(2 * p + 1) * tp + i], up_r)
+                pre.append(z + bias2)
+            return [
+                jnp.concatenate([z[k * own : (k + 1) * own] for z in pre], 0) for k in range(2)
+            ]
+
+        def decay():
+            tri = diagonal.astype(F32)
+            for p in range(fs // 2):
+                for s, z in zip((slot, far_slot), gate(p)):
+                    decay_of(s, p, z, tri)
+
+        def decay_of(s, p, z, tri):
+            rate = (jnp.minimum(z, 0.0) - jnp.log1p(jnp.exp(-jnp.abs(z)))) / SOFTMAX_TEMPER
+            within = exact(tri, rate)
+            t0, t1 = within[SPAN - 1 : SPAN], within[rows - 1 :]
+            grow = jnp.exp(within) * KEY_DIM**-0.5
+            end = jnp.exp(jnp.where(early, t0, t1) - within)
+            decays[s, p, 0] = grow
+            decays[s, p, 1] = jnp.exp(-within)
+            decays[s, p, 2] = end
+            decays[s, p, 3] = grow * jnp.where(early, 1.0, jnp.exp(t0))
+            decays[s, p, 4] = end * jnp.where(early, jnp.exp(t1), 1.0)
+            totals[s, p] = jnp.broadcast_to(jnp.exp(t0 + t1), totals.shape[2:])
+
+        def window_maps(s, slices):
+            total = nn(x_buf[s, :, columns(slices[0])], slice_rows(ww, slices[0])[...])
+            for j in slices[1:]:
+                total += nn(x_buf[s, :, columns(j)], slice_rows(ww, j)[...])
+            return total
+
+        arrive(LOW, buddy, True)
+        w_copy(STATE, me).start()
+        arrive(LOW, third, False)
+        arrive(LOW, fourth, False)
+        x_copy(far_slot, mine, 0, SIB).wait_recv()
+        start(x_first(far_slot))
+        for s in chunks[1:]:
+            low_share(s, 1 - c).wait_recv()
+        own_low()
+        start(l_first())
+        arrive(KV, third, False)
+        neighbours(slot)
+        arrive(KV, buddy, True)
+        arrive(QUERY, buddy, True)
+        for i in (b1, b2, b3):
+            l_copy(i, 0, SIB).wait_recv()
+        start(l_onward())
+        neighbours(far_slot)
+        corner(slot)
+        for g in range(fs):
+            l_copy(g * tp + 1 - c, 0, SIB).wait_recv()
+        decay()
+        arrive(STATE, buddy, True)
+        o_copy(0, me, 0).start()
+        arrive(KV, fourth, False)
+        siblings(slot)
+        arrive(QUERY, third, False)
+        for s in chunks[1:3]:
+            kv_share(s, 1 - side).wait_recv()
+        acc[slot] = window_maps(slot, chunks[:3])
+        corner(far_slot)
+        siblings(far_slot)
+        acc[far_slot] = window_maps(far_slot, chunks[:3])
+        arrive(QUERY, fourth, False)
+        kv_share(fourth, 1 - side).wait_recv()
+
+        def place(s):
+            p = acc[s] + window_maps(s, chunks[3:])
+            qw[s] = (p[:, :wq_cols].astype(BF).astype(F32) * HEAD_DIM**-0.5).astype(BF)
+            kvb[s + 1] = p[:, wq_cols:].astype(BF)
+
+        place(slot)
+        place(far_slot)
 
         @pl.when(me == 1)
         def _():
@@ -854,31 +968,9 @@
             kvb[0] = jnp.zeros(kvb.shape[1:], BF)
             state_in[...] = jnp.zeros_like(state_in)
 
-        up = jnp.where(side == 0, up_ref[:, :KEY_DIM], up_ref[:, KEY_DIM:pair])
-        up1 = jnp.where(side == 0, up_ref[:, pair : pair + KEY_DIM], up_ref[:, pair + KEY_DIM :])
-        up = jnp.where(f // 2 == 0, up, up1)
-        bs = [bias_ref[:, i * KEY_DIM : (i + 1) * KEY_DIM] for i in range(fs)]
-        bias = bs[0]
-        for i in range(1, fs):
-            bias = jnp.where(f == i, bs[i], bias)
-        up_l = jnp.concatenate([up, jnp.zeros_like(up)], 1)
-        up_r = jnp.concatenate([jnp.zeros_like(up), up], 1)
-        bias2 = jnp.concatenate([bias, bias], 1)
-        tri = diagonal.astype(F32)
-        for s in range(2):
-            for p in range(fs // 2):
-                z = nn(lowb[s, seq(2 * p)], up_l) + nn(lowb[s, seq(2 * p + 1)], up_r) + bias2
-                rate = (jnp.minimum(z, 0.0) - jnp.log1p(jnp.exp(-jnp.abs(z)))) / SOFTMAX_TEMPER
-                within = exact(tri, rate)
-                t0, t1 = within[SPAN - 1 : SPAN], within[rows - 1 :]
-                grow = jnp.exp(within) * KEY_DIM**-0.5
-                end = jnp.exp(jnp.where(early, t0, t1) - within)
-                decays[s, p, 0] = grow
-                decays[s, p, 1] = jnp.exp(-within)
-                decays[s, p, 2] = end
-                decays[s, p, 3] = grow * jnp.where(early, 1.0, jnp.exp(t0))
-                decays[s, p, 4] = end * jnp.where(early, jnp.exp(t1), 1.0)
-                totals[s, p] = jnp.broadcast_to(jnp.exp(t0 + t1), totals.shape[2:])
+        @pl.when(me > 1)
+        def _():
+            o_copy(0, me, 1).start()
 
         qi = lax.broadcasted_iota(jnp.int32, (WINDOW, 2 * WINDOW), 0)
         ki = lax.broadcasted_iota(jnp.int32, (WINDOW, 2 * WINDOW), 1)
@@ -911,18 +1003,13 @@
 
         window(far_slot)
         hid_copy(1, far_slot).start()
-        w_copy(3, third).wait_recv()
-        w_copy(3, fourth).wait_recv()
-
-        def second_maps(i, _):
-            s = i // fs
-            b = lax.rem(i, fs)
-            p = nn(x_buf[s, seq(b)], wg[...]).astype(BF)
-            gvb[s, seq(b)] = p[:, :VALUE_DIM]
-            qkb[s, seq(b)] = p[:, VALUE_DIM:].astype(F32)
-            return 0
-
-        lax.fori_loop(0, 2 * fs, second_maps, 0)
+        w_copy(STATE, third).wait_recv()
+        w_copy(STATE, fourth).wait_recv()
+
+        for s in range(2):
+            p = nn(x_buf[s], wg[...]).astype(BF)
+            gvb[s] = p[:, :VALUE_DIM]
+            qkb[s] = p[:, VALUE_DIM:].astype(F32)
 
         def keys(s, p):
             return jnp.where(left, roll_half(qkb[s, seq(2 * p)]), qkb[s, seq(2 * p + 1)])
@@ -942,9 +1029,11 @@
         @pl.when(me == 1)
         def _():
             state.start()
-
-        o_copy(0, buddy).wait_recv()
-        o_copy(0, buddy).start()
+            o_copy(0, me, 1).start()
+
+        for h in range(2):
+            o_copy(0, buddy, h).wait_recv()
+            o_copy(0, buddy, h).start()
 
         for s in range(2):
             for p in range(fs // 2):
@@ -979,6 +1068,9 @@
 
         finish_state(far_slot)
         hid_copy(0, far_slot).start()
+        for h in range(2):
+            o_copy(0, third, h).wait_recv()
+            o_copy(1, third, h).start()
         finish_state(slot)
 
         @pl.when(me > 1)
@@ -992,71 +1084,77 @@
         hid_copy(1, slot).wait_recv()
         hid_copy(0, slot).wait_recv()
 
-    nc = o_buf.shape[2]
-
-    def half_copy(s):
-        return remote(half_out.at[s], half_in.at[s], half_send.at[s], half_recv.at[s], SIB)
-
-    def piece_copy(s, d, target):
+    parts = [(s, h) for s in chunks for h in range(2)]
+
+    def half_copy(s, h):
         return remote(
-            piece_out.at[s, d - 1], piece_in.at[s, d - 1],
-            piece_send.at[s, d - 1], piece_recv.at[s, d - 1], {"fs": target},
+            half_out.at[s, h], half_in.at[s, h], half_send.at[s, h], half_recv.at[s, h], SIB
         )
 
+    def piece_copy(s, h, d, target):
+        return remote(
+            piece_out.at[s, h, d - 1], piece_in.at[s, h, d - 1],
+            piece_send.at[s, h, d - 1], piece_recv.at[s, h, d - 1], {"fs": target},
+        )
+
     def produce(t):
-        s = chunks[t]
-        if t == 1:
+        s, h = parts[t]
+        if 2 <= t < 6:
             @pl.when(outer)
             def _():
-                o_copy(0, s).wait_recv()
-        if t > 1:
-            o_copy(0, s).wait_recv()
+                o_copy(0, s, h).wait_recv()
+        if t >= 6:
+            o_copy(0, s, h).wait_recv()
 
             @pl.when(inner)
             def _():
-                o_copy(1, s).start()
-
-        w = o_buf[s]
+                o_copy(1, s, h).start()
+
+        w = o_buf[s, h]
         for b in range(fs):
             partial = nn(hidden[slot, seq(b)], w)
             lo, hi = partial[:own], partial[own:]
-            half_out[s, b] = jnp.where(c == 0, hi, lo).astype(BF)
-            half_own[s, b] = jnp.where(c == 0, lo, hi)
-        half_copy(s).start()
+            half_out[s, h, b] = jnp.where(c == 0, hi, lo).astype(BF)
+            half_own[s, h, b] = jnp.where(c == 0, lo, hi)
+        half_copy(s, h).start()
 
     def combine(t):
-        s = chunks[t]
-        half_copy(s).wait_recv()
+        s, h = parts[t]
+        half_copy(s, h).wait_recv()
         for d in range(1, fs):
             to = lax.rem(f + d, fs)
-            piece_out[s, d - 1] = (half_own[s, to] + half_in[s, to].astype(F32)).astype(BF)
-            piece_copy(s, d, to).start()
-        piece_own[s] = half_own[s, f] + half_in[s, f].astype(F32)
+            piece_out[s, h, d - 1] = (half_own[s, h, to] + half_in[s, h, to].astype(F32)).astype(BF)
+            piece_copy(s, h, d, to).start()
+        piece_own[s, h] = half_own[s, h, f] + half_in[s, h, f].astype(F32)
 
     def finish(t):
-        s = chunks[t]
-        total = piece_own[s]
+        s, h = parts[t]
+        total = piece_own[s, h]
         for d in range(1, fs):
-            piece_copy(s, d, f).wait_recv()
-            total += piece_in[s, d - 1].astype(F32)
-        out_ref[:, pl.ds(pl.multiple_of(s * nc, nc), nc)] = total.astype(BF)
+            piece_copy(s, h, d, f).wait_recv()
+            total += piece_in[s, h, d - 1].astype(F32)
+        at = pl.ds(pl.multiple_of((2 * s + h) * nc, nc), nc)
+        out_ref[:, at] = total.astype(BF)
+        pltpu.make_async_copy(out_ref.at[:, at], out_hbm.at[:, at], out_sem.at[t]).start()
 
     produce(0)
-    for t in range(1, sp):
+    for t in range(1, 2 * sp):
         produce(t)
         combine(t - 1)
-    combine(sp - 1)
-    for t in range(sp):
+    combine(2 * sp - 1)
+    for t in range(2 * sp):
         finish(t)
-    for t in range(sp):
-        s = chunks[t]
-        half_copy(s).wait_send()
+    for t, (s, h) in enumerate(parts):
+        at = pl.ds(pl.multiple_of((2 * s + h) * nc, nc), nc)
+        pltpu.make_async_copy(out_ref.at[:, at], out_hbm.at[:, at], out_sem.at[t]).wait()
+        half_copy(s, h).wait_send()
         for d in range(1, fs):
-            piece_copy(s, d, f).wait_send()
+            piece_copy(s, h, d, f).wait_send()
 
     for kind in range(4):
         w_copy(kind, me).wait_send()
-    o_copy(0, me).wait_send()
+    for h in range(2):
+        o_copy(0, me, h).wait_send()
 
     @pl.when(outer)
     def _():
@@ -1069,12 +1167,15 @@
                 copy.wait_send()
         for kind in range(4):
             w_copy(kind, buddy).wait_send()
+        for copy in l_first() + l_onward():
+            copy.wait_send()
         for s in chunks[1:]:
             kv_share(s, side).wait_send()
             low_share(s, c).wait_send()
-        o_copy(0, buddy).wait_send()
-        for s in (me, third, fourth):
-            o_copy(1, s).wait_send()
+        for h in range(2):
+            o_copy(0, buddy, h).wait_send()
+            for s in (me, third, fourth):
+                o_copy(1, s, h).wait_send()
         for i in range(2):
             hid_copy(i, far_slot).wait_send()
 
@@ -1097,18 +1198,23 @@
     pairs = fs // 2
     vm = pltpu.VMEM
     dma = pltpu.SemaphoreType.DMA
+    small = [(o.shape, o.dtype) for o in operands[10:]]
     scratch = [
+        vm((own, d), BF),
+        *(vm(shape, dtype) for shape, dtype in small),
+        vm((own, sp * nc), BF),
         vm((2, all_rows, d), BF),
         vm((d, 2 * pair), BF),
         vm((d, VALUE_DIM + pair), BF),
         vm((sp, rank, kc), BF),
-        vm((sp, depth, nc), BF),
+        vm((sp, 2, depth, nc // 2), BF),
         vm((4, kc, pair), BF),
         vm((2, all_rows, pair), BF),
         vm((3, all_rows, pair), BF),
         vm((2, all_rows, VALUE_DIM), BF),
         vm((2, all_rows, pair), F32),
-        vm((2, all_rows, rank), BF),
+        vm((2, all_rows, 2 * pair), F32),
+        vm((fs * tp, rank, 2 * own), BF),
         vm((2, pairs, 5, rows, pair), F32),
         vm((2, pairs, 8, pair), F32),
         vm((2, pairs, VALUE_DIM, pair), F32),
@@ -1117,37 +1223,39 @@
         vm((2, all_rows, VALUE_DIM), F32),
         vm((2, all_rows, pair), BF),
         vm((2, all_rows, depth), BF),
-        vm((sp, fs, own, nc), BF),
-        vm((sp, fs, own, nc), BF),
-        vm((sp, fs, own, nc), F32),
-        vm((sp, fs - 1, own, nc), BF),
-        vm((sp, fs - 1, own, nc), BF),
-        vm((sp, own, nc), F32),
-        dma((9,)),
+        vm((sp, 2, fs, own, nc // 2), BF),
+        vm((sp, 2, fs, own, nc // 2), BF),
+        vm((sp, 2, fs, own, nc // 2), F32),
+        vm((sp, 2, fs - 1, own, nc // 2), BF),
+        vm((sp, 2, fs - 1, own, nc // 2), BF),
+        vm((sp, 2, own, nc // 2), F32),
+        dma((17,)),
+        dma((2 * sp,)),
+        dma((7,)),
+        dma((fs * tp,)),
         dma((2, 7)),
         dma((2, fs * tp)),
         dma((4, sp)),
         dma((4, sp)),
         dma((2, sp)),
         dma((2, sp)),
-        dma((2, sp)),
-        dma((sp,)),
+        dma((2, sp, 2)),
+        dma((sp, 2)),
         dma((2,)),
         dma((2,)),
         dma((2,)),
         dma((2,)),
-        dma((sp,)),
-        dma((sp,)),
-        dma((sp, fs - 1)),
-        dma((sp, fs - 1)),
+        dma((sp, 2)),
+        dma((sp, 2)),
+        dma((sp, 2, fs - 1)),
+        dma((sp, 2, fs - 1)),
     ]
-    spec = pl.BlockSpec(memory_space=pltpu.VMEM)
     anywhere = pl.BlockSpec(memory_space=pl.ANY)
     return pl.pallas_call(
         functools.partial(fold_kernel, sizes),
         out_shape=jax.ShapeDtypeStruct((own, sp * nc), BF),
-        in_specs=[anywhere if i in (1, 2, 3, 4, 5, 6, 8, 9) else spec for i in range(15)],
-        out_specs=spec,
+        in_specs=[anywhere] * 15,
+        out_specs=anywhere,
         scratch_shapes=scratch,
         compiler_params=pltpu.CompilerParams(
             has_side_effects=True, vmem_limit_bytes=60 * 1024 * 1024, collective_id=0
@@ -1157,7 +1265,7 @@
 
 def folds(sp, fs, tp, shape, rows, kc, width, rank, nc, depth):
     whole_rows = rows == WINDOW == 2 * SPAN
-    lanes_fit = nc % 128 == 0 and kc % 128 == 0 and depth == 2 * VALUE_DIM
+    lanes_fit = nc % 256 == 0 and kc % 128 == 0 and depth == 2 * VALUE_DIM
     return sp == 4 and fs == 4 and tp == 2 and whole_rows and lanes_fit and rank % 32 == 0
 
 

time: 73.1 us -> 63 us (0.86); the launches traced: 72.9 us -> 62 us
  Pallas kernels: 71.3 us -> 60.3 us
    pallas_call x1, Pallas kernels: 71.3 us -> 60.3 us  [fold_call(): pl.pallas_call(functools.partial(fold_kernel, sizes), out_shape=jax.Shape...]
where the time goes in v2:
time: 63 us; the launch traced here: 62 us
  Pallas kernels  60.3 us (96%)
  local copies, waits for them, and re-layouts  1.67 us (3%)
    pallas_call x1, Pallas kernels, fold_call(): pl.pallas_call(functools.partial(fold_kernel, sizes), out_shape=jax.Shape...  60.3 us
    unnamed x1, local copies, waits for them, and re-layouts  1.67 us

profile of v2, /device:TPU:0, one launch (start us, length us, event | category | flops | bytes accessed | tf_op | source)
XLA Modules:
  0.0 62.0 jit_solution(7125222134753719920)
XLA Ops:
  0.0 60.3 %shard_map.145 = bf16[64,2048]{1,0:T(8,128)(2,1)} custom-call(bf16[64,2048]{1,0:T(8,128)(2,1)} %bitcast.8, bf16[512,512]{1,0:T(8,128)(2,1)} %gv_ref.1, bf16[512,512]{1,0:T(8,128)(2,1)} %wq_ref.1, bf16[512,256]{1,0:T(8,128)(2,1)} %gq_ref.1, bf16[512,256]{1,0:T(8,128)(2,1)} %gk_ref.1, bf16[512,128]{1,0:T(8,128)(2,1)} %wk_ref.1, bf16[512,128]{1,0:T(8,128)(2,1)} %wv_ref.1, ...), custom_call_target="tpu_custom_call" | custom-call | tf_op jit(solution)/shard_map/pallas_call | solution.py:1254
  60.3 1.7 %copy.17 = bf16[1,64,2048]{2,1,0:T(8,128)(2,1)} copy(bf16[1,64,2048]{2,1,0:T(8,128)(2,1)} %bitcast.7) | data formatting | bytes 524288

commit v3 on v2

--- a/solution.py
+++ b/solution.py
@@ -560,6 +560,9 @@
     qkb,
     acc,
     lowx,
+    fill,
+    sc,
+    ew,
     decays,
     totals,
     states,
@@ -691,9 +694,6 @@
     for copy in locals_[11:] + locals_[:11]:
         copy.start()
 
-    def block(s, i):
-        return x_buf.at[s, pl.ds(pl.multiple_of(i * own, own), own)]
-
     mine = f * tp + c
     b1, b2, b3 = n1 * tp + c, n2 * tp + c, (fs - 1 - f) * tp + c
 
@@ -702,32 +702,37 @@
     normed = rms_rows(tok_ref[...].astype(F32), ngain_ref[...]).astype(BF)
     x_buf[slot, pl.ds(pl.multiple_of(mine * own, own), own)] = normed
 
-    def x_copy(s, i, k, target):
-        return remote(block(s, i), block(s, i), x_send.at[s, k], x_recv.at[s, i], target)
+    def half_block(s, i, h):
+        at = pl.multiple_of(i * own + h * (own // 2), own // 2)
+        return x_buf.at[s, pl.ds(at, own // 2)]
+
+    def x_copy(s, i, h, k, target):
+        ref = half_block(s, i, h)
+        return remote(ref, ref, x_send.at[s, k, h], x_recv.at[s, i, h], target)
 
     SIB = {"tp": 1 - c}
 
-    def x_first(s):
+    def x_first(s, h):
         return [
-            x_copy(s, mine, 0, {"fs": n1}),
-            x_copy(s, mine, 1, {"fs": n2}),
-            x_copy(s, mine, 2, SIB),
+            x_copy(s, mine, h, 0, {"fs": n1}),
+            x_copy(s, mine, h, 1, {"fs": n2}),
+            x_copy(s, mine, h, 2, SIB),
         ]
 
-    def x_from1(s):
-        return [x_copy(s, b1, 3, {"fs": n2}), x_copy(s, b1, 4, SIB)]
-
-    def x_from2(s):
-        return [x_copy(s, b2, 5, SIB)]
-
-    def x_from3(s):
-        return [x_copy(s, b3, 6, SIB)]
-
-    def x_all(s):
-        return x_first(s) + x_from1(s) + x_from2(s) + x_from3(s)
-
-    def x_out():
-        return x_copy(slot, mine, 0, {"sp": middle})
+    def x_from1(s, h):
+        return [x_copy(s, b1, h, 3, {"fs": n2}), x_copy(s, b1, h, 4, SIB)]
+
+    def x_from2(s, h):
+        return [x_copy(s, b2, h, 5, SIB)]
+
+    def x_from3(s, h):
+        return [x_copy(s, b3, h, 6, SIB)]
+
+    def x_all(s, h):
+        return x_first(s, h) + x_from1(s, h) + x_from2(s, h) + x_from3(s, h)
+
+    def x_out(h):
+        return x_copy(slot, mine, h, 0, {"sp": middle})
 
     def kv_rows(s, h):
         at = pl.multiple_of(s * kc + h * part, part)
@@ -753,11 +758,17 @@
     def low_share(s, h):
         return remote(low_rows(s, h), low_rows(s, h), p_send.at[1, s], p_recv.at[1, s], SIB)
 
-    def o_copy(way, s, h):
+    def o_copy(way, s, h, d):
         target = {"sp": middle if way == 0 else outside}
-        return remote(
-            o_buf.at[s, h], o_buf.at[s, h], o_send.at[way, s, h], o_recv.at[s, h], target
-        )
+        ref = o_buf.at[s, h, pl.ds(d * gd, gd)]
+        return remote(ref, ref, o_send.at[way, s, h, d], o_recv.at[s, h, d], target)
+
+    def o_relay(way, s, h):
+        for d in range(2):
+            o_copy(0, s, h, d).wait_recv()
+            o_copy(way, s, h, d).start()
+
+    quarters = [(h, d) for h in range(2) for d in range(2)]
 
     def l_copy(i, k, target):
         return remote(lowx.at[i], lowx.at[i], l_send.at[k], l_recv.at[i], target)
@@ -781,11 +792,13 @@
 
     @pl.when(outer)
     def _():
-        x_out().start()
+        for h in range(2):
+            x_out(h).start()
 
     @pl.when(inner)
     def _():
-        start(x_first(slot))
+        for h in range(2):
+            start(x_first(slot, h))
 
     for copy in locals_[:6]:
         copy.wait()
@@ -808,8 +821,8 @@
     @pl.when(outer)
     def _():
         w_copy(STATE, me).start()
-        for h in range(2):
-            o_copy(0, me, h).start()
+        for h, d in quarters:
+            o_copy(0, me, h, d).start()
 
     lane = lax.broadcasted_iota(jnp.int32, (rows, pair), 1)
     row = lax.broadcasted_iota(jnp.int32, (rows, pair), 0)
@@ -819,7 +832,18 @@
     diagonal = same & (row >= lane)
     below = (row >= SPAN) & (lane < SPAN)
 
-    edge = remote(kvb.at[2], kvb.at[0], edge_sem.at[0], edge_sem.at[1], {"sp": me + 1})
+    def edge_rows(i, h):
+        n = fs * rows // 2
+        return kvb.at[i, pl.ds(pl.multiple_of(h * n, n), n)]
+
+    edge = remote(
+        edge_rows(2, side), edge_rows(0, side), edge_sem.at[0], edge_sem.at[1], {"sp": me + 1}
+    )
+
+    def edge_share(h):
+        return remote(
+            edge_rows(0, h), edge_rows(0, h), edge_sem.at[2], edge_sem.at[3], {"fs": xn}
+        )
     state = remote(state_out, state_in, state_sem.at[0], state_sem.at[1], {"sp": me + 1})
 
     def hid_part(s, i):
@@ -837,8 +861,8 @@
 
     @pl.when(inner)
     def _():
-        for h in range(2):
-            o_copy(1, me, h).start()
+        for h, d in quarters:
+            o_copy(1, me, h, d).start()
 
         def arrive(kind, s, onward):
             w_copy(kind, s).wait_recv()
@@ -849,19 +873,21 @@
             if kind == KV:
                 kv_share(s, side).start()
 
-        def neighbours(s):
-            x_copy(s, b1, 0, SIB).wait_recv()
-            start(x_from1(s))
-            x_copy(s, b2, 0, SIB).wait_recv()
-            start(x_from2(s))
+        def neighbours(s, h):
+            x_copy(s, b1, h, 0, SIB).wait_recv()
+            start(x_from1(s, h))
+            x_copy(s, b2, h, 0, SIB).wait_recv()
+            start(x_from2(s, h))
 
         def corner(s):
-            x_copy(s, b3, 0, SIB).wait_recv()
-            start(x_from3(s))
+            for h in range(2):
+                x_copy(s, b3, h, 0, SIB).wait_recv()
+                start(x_from3(s, h))
 
         def siblings(s):
             for g in range(fs):
-                x_copy(s, g * tp + 1 - c, 0, SIB).wait_recv()
+                for h in range(2):
+                    x_copy(s, g * tp + 1 - c, h, 0, SIB).wait_recv()
 
         def columns(s):
             return pl.ds(pl.multiple_of(s * kc, kc), kc)
@@ -918,49 +944,60 @@
                 total += nn(x_buf[s, :, columns(j)], slice_rows(ww, j)[...])
             return total
 
+        def far_rows(h):
+            x_copy(far_slot, mine, h, 0, SIB).wait_recv()
+            start(x_first(far_slot, h))
+
         arrive(LOW, buddy, True)
         w_copy(STATE, me).start()
+        o_copy(0, me, 0, 0).start()
         arrive(LOW, third, False)
+        arrive(KV, third, False)
+        neighbours(slot, 0)
+        far_rows(0)
         arrive(LOW, fourth, False)
-        x_copy(far_slot, mine, 0, SIB).wait_recv()
-        start(x_first(far_slot))
+        neighbours(slot, 1)
+        far_rows(1)
         for s in chunks[1:]:
             low_share(s, 1 - c).wait_recv()
         own_low()
         start(l_first())
-        arrive(KV, third, False)
-        neighbours(slot)
         arrive(KV, buddy, True)
+        neighbours(far_slot, 0)
         arrive(QUERY, buddy, True)
+        o_copy(0, me, 0, 1).start()
+        corner(slot)
+        siblings(slot)
+        arrive(QUERY, third, False)
+        kv_share(third, 1 - side).wait_recv()
+        acc[slot] = window_maps(slot, (me, third))
+        neighbours(far_slot, 1)
+        arrive(STATE, buddy, True)
+        arrive(KV, fourth, False)
         for i in (b1, b2, b3):
             l_copy(i, 0, SIB).wait_recv()
         start(l_onward())
-        neighbours(far_slot)
-        corner(slot)
+        o_relay(1, third, 0)
         for g in range(fs):
             l_copy(g * tp + 1 - c, 0, SIB).wait_recv()
         decay()
-        arrive(STATE, buddy, True)
-        o_copy(0, me, 0).start()
-        arrive(KV, fourth, False)
-        siblings(slot)
-        arrive(QUERY, third, False)
-        for s in chunks[1:3]:
-            kv_share(s, 1 - side).wait_recv()
-        acc[slot] = window_maps(slot, chunks[:3])
         corner(far_slot)
+        kv_share(buddy, 1 - side).wait_recv()
         siblings(far_slot)
         acc[far_slot] = window_maps(far_slot, chunks[:3])
         arrive(QUERY, fourth, False)
         kv_share(fourth, 1 - side).wait_recv()
 
-        def place(s):
-            p = acc[s] + window_maps(s, chunks[3:])
-            qw[s] = (p[:, :wq_cols].astype(BF).astype(F32) * HEAD_DIM**-0.5).astype(BF)
+        def place(s, slices):
+            p = acc[s] + window_maps(s, slices)
+            q = p[:, :wq_cols].astype(BF).astype(F32) * HEAD_DIM**-0.5
+            for h in range(heads):
+                qh = jnp.where(left_all, q if h == 0 else roll_half(q), 0.0)
+                qw[s, h] = qh.astype(BF)
             kvb[s + 1] = p[:, wq_cols:].astype(BF)
 
-        place(slot)
-        place(far_slot)
+        left_all = lax.broadcasted_iota(jnp.int32, (fs * rows, pair), 1) < KEY_DIM
+        place(slot, (buddy, fourth))
 
         @pl.when(me == 1)
         def _():
@@ -968,46 +1005,65 @@
             kvb[0] = jnp.zeros(kvb.shape[1:], BF)
             state_in[...] = jnp.zeros_like(state_in)
 
+        o_copy(0, me, 1, 0).start()
+
         @pl.when(me > 1)
         def _():
-            o_copy(0, me, 1).start()
-
-        qi = lax.broadcasted_iota(jnp.int32, (WINDOW, 2 * WINDOW), 0)
-        ki = lax.broadcasted_iota(jnp.int32, (WINDOW, 2 * WINDOW), 1)
-        distance = qi + WINDOW - ki
+            o_copy(0, me, 1, 1).start()
+
+        place(far_slot, (fourth,))
+
+        tall = heads * WINDOW
+        qi = lax.broadcasted_iota(jnp.int32, (tall, 2 * WINDOW), 0)
+        ki = lax.broadcasted_iota(jnp.int32, (tall, 2 * WINDOW), 1)
+        distance = lax.rem(qi, WINDOW) + WINDOW - ki
         inside = (distance >= 0) & (distance < WINDOW)
         sinks = sink_ref[:, :heads]
         for i in range(1, fs):
             sinks = jnp.where(f == i, sink_ref[:, i * heads : (i + 1) * heads], sinks)
+        sink = sinks[:, :1]
+        for h in range(1, heads):
+            sink = jnp.where(qi < h * WINDOW, sink, sinks[:, h : h + 1])
+        fill[...] = jnp.where(ki == 0, sink, -1e30)
+        key_row = lax.broadcasted_iota(jnp.int32, (2 * WINDOW, pair), 0)
+        key_lane = lax.broadcasted_iota(jnp.int32, (2 * WINDOW, pair), 1)
 
         def window(s):
             valid = inside & ((ki >= WINDOW) | (me > 1) | (s > 0))
-
-            def one(b, _):
-                band = jnp.concatenate([kvb[s, seq(b)], kvb[s + 1, seq(b)]], 0)
-                q = qw[s, seq(b)].astype(F32)
-                outs = []
-                for h in range(heads):
-                    qh = jnp.where(left, q if h == 0 else roll_half(q), 0.0).astype(BF)
-                    sc = jnp.where(valid, nt(qh, band), -1e30)
-                    sink = sinks[:, h : h + 1]
-                    top = jnp.maximum(jnp.max(sc, -1, keepdims=True), sink)
-                    e = jnp.exp(sc - top)
-                    den = jnp.sum(e, -1, keepdims=True) + jnp.exp(sink - top)
-                    outs.append(nn((e * (1.0 / den)).astype(BF), band))
-                hidden[s, seq(b), VALUE_DIM:] = jnp.where(left, roll_half(outs[0]), outs[1]).astype(BF)
-                return 0
-
+            bands = [jnp.concatenate([kvb[s, seq(b)], kvb[s + 1, seq(b)]], 0) for b in range(fs)]
             for b in range(fs):
-                one(b, 0)
+                q = jnp.concatenate([qw[s, h, seq(b)] for h in range(heads)], 0)
+                sc[b] = jnp.where(valid, nt(q, bands[b]), fill[...])
+            for b in range(fs):
+                near = sc[b]
+                top = jnp.max(near, -1, keepdims=True)
+                ew[b] = jnp.exp(near - top).astype(BF)
+            for b in range(fs):
+                band = jnp.concatenate([kvb[s, seq(b)], kvb[s + 1, seq(b)]], 0).astype(F32)
+                values = jnp.where(
+                    key_lane < HEAD_DIM, 1.0, jnp.where(key_row == 0, 0.0, band)
+                ).astype(BF)
+                both = nn(ew[b], values)
+                turned = roll_half(both)
+                first = turned[:WINDOW] / both[:WINDOW]
+                second = both[WINDOW:] / turned[WINDOW:]
+                hidden[s, seq(b), VALUE_DIM:] = jnp.where(left, first, second).astype(BF)
 
         window(far_slot)
         hid_copy(1, far_slot).start()
+        def state_maps(s, slices):
+            total = nn(x_buf[s, :, columns(slices[0])], slice_rows(wg, slices[0])[...])
+            for j in slices[1:]:
+                total += nn(x_buf[s, :, columns(j)], slice_rows(wg, j)[...])
+            return total
+
         w_copy(STATE, third).wait_recv()
+        for s in range(2):
+            acc[s] = state_maps(s, chunks[:3])
         w_copy(STATE, fourth).wait_recv()
 
         for s in range(2):
-            p = nn(x_buf[s], wg[...]).astype(BF)
+            p = (acc[s] + state_maps(s, chunks[3:])).astype(BF)
             gvb[s] = p[:, :VALUE_DIM]
             qkb[s] = p[:, VALUE_DIM:].astype(F32)
 
@@ -1029,11 +1085,10 @@
         @pl.when(me == 1)
         def _():
             state.start()
-            o_copy(0, me, 1).start()
+            o_copy(0, me, 1, 1).start()
 
         for h in range(2):
-            o_copy(0, buddy, h).wait_recv()
-            o_copy(0, buddy, h).start()
+            o_relay(0, buddy, h)
 
         for s in range(2):
             for p in range(fs // 2):
@@ -1054,6 +1109,8 @@
 
         @pl.when(me > 1)
         def _():
+            edge.wait_recv()
+            edge_share(side).start()
             state.wait_recv()
 
         def finish_state(s):
@@ -1068,16 +1125,14 @@
 
         finish_state(far_slot)
         hid_copy(0, far_slot).start()
-        for h in range(2):
-            o_copy(0, third, h).wait_recv()
-            o_copy(1, third, h).start()
         finish_state(slot)
 
         @pl.when(me > 1)
         def _():
-            edge.wait_recv()
+            edge_share(1 - side).wait_recv()
 
         window(slot)
+        o_relay(1, third, 1)
 
     @pl.when(outer)
     def _():
@@ -1102,13 +1157,15 @@
         if 2 <= t < 6:
             @pl.when(outer)
             def _():
-                o_copy(0, s, h).wait_recv()
+                for d in range(2):
+                    o_copy(0, s, h, d).wait_recv()
         if t >= 6:
-            o_copy(0, s, h).wait_recv()
-
-            @pl.when(inner)
-            def _():
-                o_copy(1, s, h).start()
+            for d in range(2):
+                o_copy(0, s, h, d).wait_recv()
+
+                @pl.when(inner)
+                def _():
+                    o_copy(1, s, h, d).start()
 
         w = o_buf[s, h]
         for b in range(fs):
@@ -1153,17 +1210,18 @@
 
     for kind in range(4):
         w_copy(kind, me).wait_send()
-    for h in range(2):
-        o_copy(0, me, h).wait_send()
+    for h, d in quarters:
+        o_copy(0, me, h, d).wait_send()
 
     @pl.when(outer)
     def _():
-        x_out().wait_send()
+        for h in range(2):
+            x_out(h).wait_send()
 
     @pl.when(inner)
     def _():
         for s in range(2):
-            for copy in x_all(s):
+            for copy in x_all(s, 0) + x_all(s, 1):
                 copy.wait_send()
         for kind in range(4):
             w_copy(kind, buddy).wait_send()
@@ -1172,10 +1230,10 @@
         for s in chunks[1:]:
             kv_share(s, side).wait_send()
             low_share(s, c).wait_send()
-        for h in range(2):
-            o_copy(0, buddy, h).wait_send()
+        for h, d in quarters:
+            o_copy(0, buddy, h, d).wait_send()
             for s in (me, third, fourth):
-                o_copy(1, s, h).wait_send()
+                o_copy(1, s, h, d).wait_send()
         for i in range(2):
             hid_copy(i, far_slot).wait_send()
 
@@ -1183,6 +1241,10 @@
         def _():
             edge.wait_send()
             state.wait_send()
+
+        @pl.when(me > 1)
+        def _():
+            edge_share(side).wait_send()
 
 
 def fold_call(sizes, operands):
@@ -1209,12 +1271,15 @@
         vm((sp, rank, kc), BF),
         vm((sp, 2, depth, nc // 2), BF),
         vm((4, kc, pair), BF),
-        vm((2, all_rows, pair), BF),
+        vm((2, 2, all_rows, pair), BF),
         vm((3, all_rows, pair), BF),
         vm((2, all_rows, VALUE_DIM), BF),
         vm((2, all_rows, pair), F32),
         vm((2, all_rows, 2 * pair), F32),
         vm((fs * tp, rank, 2 * own), BF),
+        vm((2 * WINDOW, 2 * WINDOW), F32),
+        vm((fs, 2 * WINDOW, 2 * WINDOW), F32),
+        vm((fs, 2 * WINDOW, 2 * WINDOW), BF),
         vm((2, pairs, 5, rows, pair), F32),
         vm((2, pairs, 8, pair), F32),
         vm((2, pairs, VALUE_DIM, pair), F32),
@@ -1233,15 +1298,15 @@
         dma((2 * sp,)),
         dma((7,)),
         dma((fs * tp,)),
-        dma((2, 7)),
-        dma((2, fs * tp)),
+        dma((2, 7, 2)),
+        dma((2, fs * tp, 2)),
         dma((4, sp)),
         dma((4, sp)),
         dma((2, sp)),
         dma((2, sp)),
-        dma((2, sp, 2)),
-        dma((sp, 2)),
-        dma((2,)),
+        dma((2, sp, 2, 2)),
+        dma((sp, 2, 2)),
+        dma((4,)),
         dma((2,)),
         dma((2,)),
         dma((2,)),
@@ -1265,7 +1330,7 @@
 
 def folds(sp, fs, tp, shape, rows, kc, width, rank, nc, depth):
     whole_rows = rows == WINDOW == 2 * SPAN
-    lanes_fit = nc % 256 == 0 and kc % 128 == 0 and depth == 2 * VALUE_DIM
+    lanes_fit = nc % 256 == 0 and kc % 128 == 0 and depth == 2 * VALUE_DIM and 2 * HEAD_DIM == 2 * KEY_DIM
     return sp == 4 and fs == 4 and tp == 2 and whole_rows and lanes_fit and rank % 32 == 0
 
 

time: 63 us -> 58.3 us (0.925); the launches traced: 62 us -> 58.1 us
  Pallas kernels: 60.3 us -> 56.4 us
    pallas_call x1, Pallas kernels: 60.3 us -> 56.4 us  [fold_call(): pl.pallas_call(functools.partial(fold_kernel, sizes), out_shape=jax.Shape...]
where the time goes in v3:
time: 58.3 us; the launch traced here: 58.1 us
  Pallas kernels  56.4 us (97%)
  local copies, waits for them, and re-layouts  1.67 us (3%)
    pallas_call x1, Pallas kernels, fold_call(): pl.pallas_call(functools.partial(fold_kernel, sizes), out_shape=jax.Shape...  56.4 us
    unnamed x1, local copies, waits for them, and re-layouts  1.67 us

profile of v3, /device:TPU:0, one launch (start us, length us, event | category | flops | bytes accessed | tf_op | source)
XLA Modules:
  0.0 58.1 jit_solution(2072273728366531873)
XLA Ops:
  0.0 56.4 %shard_map.145 = bf16[64,2048]{1,0:T(8,128)(2,1)} custom-call(bf16[64,2048]{1,0:T(8,128)(2,1)} %bitcast.8, bf16[512,512]{1,0:T(8,128)(2,1)} %gv_ref.1, bf16[512,512]{1,0:T(8,128)(2,1)} %wq_ref.1, bf16[512,256]{1,0:T(8,128)(2,1)} %gq_ref.1, bf16[512,256]{1,0:T(8,128)(2,1)} %gk_ref.1, bf16[512,128]{1,0:T(8,128)(2,1)} %wk_ref.1, bf16[512,128]{1,0:T(8,128)(2,1)} %wv_ref.1, ...), custom_call_target="tpu_custom_call" | custom-call | tf_op jit(solution)/shard_map/pallas_call | solution.py:1319
  56.4 1.7 %copy.17 = bf16[1,64,2048]{2,1,0:T(8,128)(2,1)} copy(bf16[1,64,2048]{2,1,0:T(8,128)(2,1)} %bitcast.7) | data formatting | bytes 524288

commit v4 on v3

--- a/solution.py
+++ b/solution.py
@@ -540,14 +540,13 @@
     bias_in,
     hgain_in,
     sink_in,
-    out_hbm,
+    out_ref,
     tok_ref,
     ngain_ref,
     up_ref,
     bias_ref,
     hgain_ref,
     sink_ref,
-    out_ref,
     x_buf,
     ww,
     wg,
@@ -559,6 +558,9 @@
     gvb,
     qkb,
     acc,
+    acc2,
+    og,
+    hall,
     lowx,
     fill,
     sc,
@@ -578,11 +580,11 @@
     piece_in,
     piece_own,
     local_sem,
-    out_sem,
     l_send,
     l_recv,
     x_send,
     x_recv,
+    x_share,
     w_send,
     w_recv,
     p_send,
@@ -597,6 +599,11 @@
     half_recv,
     piece_send,
     piece_recv,
+    g_send,
+    g_recv,
+    g_rest,
+    a_send,
+    a_recv,
 ):
     sp, fs, tp = sizes
     me = lax.axis_index("sp")
@@ -688,9 +695,14 @@
         (hgain_in, hgain_ref),
         (sink_in, sink_ref),
     ]
+    shared = [0, 0, 0, 0, 1, 2, 3, 4, 4, 4, 4] + list(range(5, 11))
     locals_ = [
-        pltpu.make_async_copy(a, b, local_sem.at[i]) for i, (a, b) in enumerate(copies_in)
+        pltpu.make_async_copy(a, b, local_sem.at[i]) for i, (a, b) in zip(shared, copies_in)
     ]
+
+    def local_wait(ref, i):
+        pltpu.make_async_copy(ref, ref, local_sem.at[i]).wait()
+
     for copy in locals_[11:] + locals_[:11]:
         copy.start()
 
@@ -706,33 +718,32 @@
         at = pl.multiple_of(i * own + h * (own // 2), own // 2)
         return x_buf.at[s, pl.ds(at, own // 2)]
 
-    def x_copy(s, i, h, k, target):
+    def x_copy(s, i, h, target, src):
         ref = half_block(s, i, h)
-        return remote(ref, ref, x_send.at[s, k, h], x_recv.at[s, i, h], target)
+        return remote(ref, ref, x_send.at[s], x_recv.at[s, src, h], target)
+
+    def x_sib(s, i, h):
+        ref = half_block(s, i, h)
+        return remote(ref, ref, x_send.at[s], x_share.at[s], SIB)
+
+    def x_bulk(s, n):
+        ref = x_buf.at[s, pl.ds(0, n * (own // 2))]
+        return remote(ref, ref, x_send.at[s], x_share.at[s], SIB)
 
     SIB = {"tp": 1 - c}
 
     def x_first(s, h):
         return [
-            x_copy(s, mine, h, 0, {"fs": n1}),
-            x_copy(s, mine, h, 1, {"fs": n2}),
-            x_copy(s, mine, h, 2, SIB),
+            x_copy(s, mine, h, {"fs": n1}, 1),
+            x_copy(s, mine, h, {"fs": n2}, 2),
+            x_sib(s, mine, h),
         ]
 
     def x_from1(s, h):
-        return [x_copy(s, b1, h, 3, {"fs": n2}), x_copy(s, b1, h, 4, SIB)]
-
-    def x_from2(s, h):
-        return [x_copy(s, b2, h, 5, SIB)]
-
-    def x_from3(s, h):
-        return [x_copy(s, b3, h, 6, SIB)]
-
-    def x_all(s, h):
-        return x_first(s, h) + x_from1(s, h) + x_from2(s, h) + x_from3(s, h)
+        return [x_copy(s, b1, h, {"fs": n2}, 3), x_sib(s, b1, h)]
 
     def x_out(h):
-        return x_copy(slot, mine, h, 0, {"sp": middle})
+        return x_copy(slot, mine, h, {"sp": middle}, 0)
 
     def kv_rows(s, h):
         at = pl.multiple_of(s * kc + h * part, part)
@@ -748,20 +759,35 @@
             lambda: low_rows(s, c),
             lambda: slice_rows(wg, s),
         )[kind]()
-        return remote(ref, ref, w_send.at[kind, s], w_recv.at[kind, s], {"sp": middle})
+        return remote(ref, ref, w_send.at[kind], w_recv.at[kind, s], {"sp": middle})
+
+    def w_bulk(kind, n):
+        ref = (
+            lambda: ww.at[pl.ds(0, n * kc), :wq_cols],
+            lambda: ww.at[pl.ds(0, n * part), wq_cols:],
+            lambda: wl.at[0, pl.ds(0, n * lpart)],
+            lambda: wg.at[pl.ds(0, n * kc)],
+        )[kind]()
+        return remote(ref, ref, w_send.at[kind], w_recv.at[kind, 0], {"sp": middle})
 
     def kv_share(s, h):
-        return remote(
-            kv_rows(s, h), kv_rows(s, h), p_send.at[0, s], p_recv.at[0, s], {"fs": xn}
-        )
+        return remote(kv_rows(s, h), kv_rows(s, h), p_send.at[0], p_recv.at[s], {"fs": xn})
 
     def low_share(s, h):
-        return remote(low_rows(s, h), low_rows(s, h), p_send.at[1, s], p_recv.at[1, s], SIB)
+        return remote(low_rows(s, h), low_rows(s, h), p_send.at[1], p_recv.at[sp], SIB)
+
+    def share_bulk(i):
+        ref = ww.at[pl.ds(0, 3 * part), wq_cols:] if i == 0 else wl.at[pl.ds(0, 3), pl.ds(0, lpart)]
+        return remote(ref, ref, p_send.at[i], p_recv.at[sp], SIB)
 
     def o_copy(way, s, h, d):
         target = {"sp": middle if way == 0 else outside}
         ref = o_buf.at[s, h, pl.ds(d * gd, gd)]
-        return remote(ref, ref, o_send.at[way, s, h, d], o_recv.at[s, h, d], target)
+        return remote(ref, ref, o_send.at[way], o_recv.at[s, h, d], target)
+
+    def o_bulk(way, n):
+        ref = o_buf.at[pl.ds(0, n)]
+        return remote(ref, ref, o_send.at[way], o_recv.at[0, 0, 0], {"sp": middle})
 
     def o_relay(way, s, h):
         for d in range(2):
@@ -771,11 +797,14 @@
     quarters = [(h, d) for h in range(2) for d in range(2)]
 
     def l_copy(i, k, target):
-        return remote(lowx.at[i], lowx.at[i], l_send.at[k], l_recv.at[i], target)
+        return remote(lowx.at[i], lowx.at[i], l_send.at[0], l_recv.at[min(k // 3, 1)], target)
 
     def l_first():
         peers = [{"fs": n1}, {"fs": n2}, {"fs": fs - 1 - f}, SIB]
         return [l_copy(mine, k, peer) for k, peer in enumerate(peers)]
+
+    def l_bulk(n, which):
+        return remote(lowx.at[pl.ds(0, n)], lowx.at[pl.ds(0, n)], l_send.at[0], l_recv.at[which], SIB)
 
     def l_onward():
         return [l_copy(i, 4 + k, SIB) for k, i in enumerate((b1, b2, b3))]
@@ -800,7 +829,8 @@
         for h in range(2):
             start(x_first(slot, h))
 
-    for copy in locals_[:6]:
+    local_wait(tiles, 0)
+    for copy in locals_[4:6]:
         copy.wait()
     own_rows = pl.ds(pl.multiple_of(me * kc, kc), kc)
 
@@ -815,8 +845,7 @@
     wg[own_rows, VALUE_DIM:] = jnp.concatenate(
         [half_of(0, KEY_DIM, side), half_of(1, KEY_DIM, side)], 1
     )
-    for copy in locals_[7:11]:
-        copy.wait()
+    local_wait(o_buf.at[me], 4)
 
     @pl.when(outer)
     def _():
@@ -874,20 +903,18 @@
                 kv_share(s, side).start()
 
         def neighbours(s, h):
-            x_copy(s, b1, h, 0, SIB).wait_recv()
+            x_copy(s, b1, h, SIB, 1).wait_recv()
             start(x_from1(s, h))
-            x_copy(s, b2, h, 0, SIB).wait_recv()
-            start(x_from2(s, h))
+            x_copy(s, b2, h, SIB, 2).wait_recv()
+            x_sib(s, b2, h).start()
 
         def corner(s):
             for h in range(2):
-                x_copy(s, b3, h, 0, SIB).wait_recv()
-                start(x_from3(s, h))
+                x_copy(s, b3, h, SIB, 3).wait_recv()
+                x_sib(s, b3, h).start()
 
         def siblings(s):
-            for g in range(fs):
-                for h in range(2):
-                    x_copy(s, g * tp + 1 - c, h, 0, SIB).wait_recv()
+            x_bulk(s, 2 * fs).wait_recv()
 
         def columns(s):
             return pl.ds(pl.multiple_of(s * kc, kc), kc)
@@ -944,8 +971,42 @@
                 total += nn(x_buf[s, :, columns(j)], slice_rows(ww, j)[...])
             return total
 
+        def state_maps(s, slices):
+            total = nn(x_buf[s, :, columns(slices[0])], slice_rows(wg, slices[0])[...])
+            for j in slices[1:]:
+                total += nn(x_buf[s, :, columns(j)], slice_rows(wg, j)[...])
+            return total
+
+        def place(s, p):
+            q = p[:, :wq_cols].astype(BF).astype(F32) * HEAD_DIM**-0.5
+            for h in range(heads):
+                qh = jnp.where(left_all, q if h == 0 else roll_half(q), 0.0)
+                qw[s, h] = qh.astype(BF)
+            kvb[s + 1] = p[:, wq_cols:].astype(BF)
+
+        left_all = lax.broadcasted_iota(jnp.int32, (fs * rows, pair), 1) < KEY_DIM
+        tall = heads * WINDOW
+        qi = lax.broadcasted_iota(jnp.int32, (tall, 2 * WINDOW), 0)
+        ki = lax.broadcasted_iota(jnp.int32, (tall, 2 * WINDOW), 1)
+        distance = lax.rem(qi, WINDOW) + WINDOW - ki
+        inside = (distance >= 0) & (distance < WINDOW)
+        sinks = sink_ref[:, :heads]
+        for i in range(1, fs):
+            sinks = jnp.where(f == i, sink_ref[:, i * heads : (i + 1) * heads], sinks)
+        sink = sinks[:, :1]
+        for h in range(1, heads):
+            sink = jnp.where(qi < h * WINDOW, sink, sinks[:, h : h + 1])
+        fill[...] = jnp.where(ki == 0, sink, -1e30)
+        key_row = lax.broadcasted_iota(jnp.int32, (2 * WINDOW, pair), 0)
+        key_lane = lax.broadcasted_iota(jnp.int32, (2 * WINDOW, pair), 1)
+
+        @pl.when(me == 1)
+        def _():
+            kvb[0] = jnp.zeros(kvb.shape[1:], BF)
+            state_in[...] = jnp.zeros_like(state_in)
+
         def far_rows(h):
-            x_copy(far_slot, mine, h, 0, SIB).wait_recv()
+            x_copy(far_slot, mine, h, SIB, 0).wait_recv()
             start(x_first(far_slot, h))
 
         arrive(LOW, buddy, True)
@@ -958,8 +1019,7 @@
         arrive(LOW, fourth, False)
         neighbours(slot, 1)
         far_rows(1)
-        for s in chunks[1:]:
-            low_share(s, 1 - c).wait_recv()
+        share_bulk(1).wait_recv()
         own_low()
         start(l_first())
         arrive(KV, buddy, True)
@@ -974,59 +1034,32 @@
         neighbours(far_slot, 1)
         arrive(STATE, buddy, True)
         arrive(KV, fourth, False)
-        for i in (b1, b2, b3):
-            l_copy(i, 0, SIB).wait_recv()
+        l_bulk(3, 0).wait_recv()
         start(l_onward())
+        l_bulk(4, 1).wait_recv()
+        decay()
+        w_copy(STATE, third).wait_recv()
+        acc2[slot] = state_maps(slot, chunks[:3])
         o_relay(1, third, 0)
-        for g in range(fs):
-            l_copy(g * tp + 1 - c, 0, SIB).wait_recv()
-        decay()
         corner(far_slot)
+        arrive(QUERY, fourth, False)
         kv_share(buddy, 1 - side).wait_recv()
+        kv_share(fourth, 1 - side).wait_recv()
+
+        place(slot, acc[slot] + window_maps(slot, (buddy, fourth)))
+
+        @pl.when(me == 1)
+        def _():
+            edge.start()
+
+        o_copy(0, me, 1, 0).start()
+
+        @pl.when(me > 1)
+        def _():
+            o_copy(0, me, 1, 1).start()
+
         siblings(far_slot)
-        acc[far_slot] = window_maps(far_slot, chunks[:3])
-        arrive(QUERY, fourth, False)
-        kv_share(fourth, 1 - side).wait_recv()
-
-        def place(s, slices):
-            p = acc[s] + window_maps(s, slices)
-            q = p[:, :wq_cols].astype(BF).astype(F32) * HEAD_DIM**-0.5
-            for h in range(heads):
-                qh = jnp.where(left_all, q if h == 0 else roll_half(q), 0.0)
-                qw[s, h] = qh.astype(BF)
-            kvb[s + 1] = p[:, wq_cols:].astype(BF)
-
-        left_all = lax.broadcasted_iota(jnp.int32, (fs * rows, pair), 1) < KEY_DIM
-        place(slot, (buddy, fourth))
-
-        @pl.when(me == 1)
-        def _():
-            edge.start()
-            kvb[0] = jnp.zeros(kvb.shape[1:], BF)
-            state_in[...] = jnp.zeros_like(state_in)
-
-        o_copy(0, me, 1, 0).start()
-
-        @pl.when(me > 1)
-        def _():
-            o_copy(0, me, 1, 1).start()
-
-        place(far_slot, (fourth,))
-
-        tall = heads * WINDOW
-        qi = lax.broadcasted_iota(jnp.int32, (tall, 2 * WINDOW), 0)
-        ki = lax.broadcasted_iota(jnp.int32, (tall, 2 * WINDOW), 1)
-        distance = lax.rem(qi, WINDOW) + WINDOW - ki
-        inside = (distance >= 0) & (distance < WINDOW)
-        sinks = sink_ref[:, :heads]
-        for i in range(1, fs):
-            sinks = jnp.where(f == i, sink_ref[:, i * heads : (i + 1) * heads], sinks)
-        sink = sinks[:, :1]
-        for h in range(1, heads):
-            sink = jnp.where(qi < h * WINDOW, sink, sinks[:, h : h + 1])
-        fill[...] = jnp.where(ki == 0, sink, -1e30)
-        key_row = lax.broadcasted_iota(jnp.int32, (2 * WINDOW, pair), 0)
-        key_lane = lax.broadcasted_iota(jnp.int32, (2 * WINDOW, pair), 1)
+        place(far_slot, window_maps(far_slot, chunks))
 
         def window(s):
             valid = inside & ((ki >= WINDOW) | (me > 1) | (s > 0))
@@ -1051,19 +1084,17 @@
 
         window(far_slot)
         hid_copy(1, far_slot).start()
-        def state_maps(s, slices):
-            total = nn(x_buf[s, :, columns(slices[0])], slice_rows(wg, slices[0])[...])
-            for j in slices[1:]:
-                total += nn(x_buf[s, :, columns(j)], slice_rows(wg, j)[...])
-            return total
-
-        w_copy(STATE, third).wait_recv()
+        acc2[far_slot] = state_maps(far_slot, chunks[:3])
+
+        @pl.when(me > 1)
+        def _():
+            edge.wait_recv()
+            edge_share(side).start()
+
+        w_copy(STATE, fourth).wait_recv()
+
         for s in range(2):
-            acc[s] = state_maps(s, chunks[:3])
-        w_copy(STATE, fourth).wait_recv()
-
-        for s in range(2):
-            p = (acc[s] + state_maps(s, chunks[3:])).astype(BF)
+            p = (acc2[s] + state_maps(s, chunks[3:])).astype(BF)
             gvb[s] = p[:, :VALUE_DIM]
             qkb[s] = p[:, VALUE_DIM:].astype(F32)
 
@@ -1085,10 +1116,6 @@
         @pl.when(me == 1)
         def _():
             state.start()
-            o_copy(0, me, 1, 1).start()
-
-        for h in range(2):
-            o_relay(0, buddy, h)
 
         for s in range(2):
             for p in range(fs // 2):
@@ -1107,10 +1134,17 @@
                     local_out[s, seq(2 * p + j)] = nn(scores, gvb[s, seq(2 * p + j)])
                     q_far[s, seq(2 * p + j)] = jnp.where(here, qf, 0.0).astype(BF)
 
+        @pl.when(me == 1)
+        def _():
+            o_copy(0, me, 1, 1).start()
+
+        for h in range(2):
+            o_relay(0, buddy, h)
+
         @pl.when(me > 1)
         def _():
-            edge.wait_recv()
-            edge_share(side).start()
+            edge_share(1 - side).wait_recv()
+            window(slot)
             state.wait_recv()
 
         def finish_state(s):
@@ -1127,34 +1161,77 @@
         hid_copy(0, far_slot).start()
         finish_state(slot)
 
-        @pl.when(me > 1)
-        def _():
-            edge_share(1 - side).wait_recv()
-
-        window(slot)
-        o_relay(1, third, 1)
+        @pl.when(me == 1)
+        def _():
+            window(slot)
+
+    def g_copy(k, j, g, h, target):
+        ref = og.at[j, g, h]
+        into = g_recv.at[j, h] if k == 0 else g_rest.at[0]
+        return remote(ref, ref, g_send.at[0], into, target)
+
+    def g_bulk(n, ssem):
+        ref = og.at[:, pl.ds(0, n)]
+        return remote(ref, ref, ssem.at[0], g_rest.at[0], SIB)
+
+    corner_f = fs - 1 - f
+
+    def g_first(j, h):
+        return [g_copy(0, j, f, h, {"fs": n1}), g_copy(1, j, f, h, {"fs": n2})]
+
+    def g_relay(j, h):
+        return g_copy(2, j, n1, h, {"fs": n2})
+
+    def a_part(g, i):
+        return hidden.at[slot, seq(g), i * VALUE_DIM : (i + 1) * VALUE_DIM]
+
+    def a_copy(k, i):
+        g = (n1, n2, corner_f)[k]
+        here = hall.at[f, :, i * VALUE_DIM : (i + 1) * VALUE_DIM]
+        return remote(a_part(g, i), here, a_send.at[0], a_recv.at[0], {"fs": g})
+
+    def a_bulk():
+        ref = hall.at[pl.ds(0, fs - 1)]
+        return remote(ref, ref, a_send.at[0], a_recv.at[0], {"fs": n1})
 
     @pl.when(outer)
     def _():
-        hid_copy(1, slot).wait_recv()
-        hid_copy(0, slot).wait_recv()
+        for h in range(2):
+            og[0, f, h] = o_buf[me, h]
+            start(g_first(0, h))
+        for h in range(2):
+            for d in range(2):
+                o_copy(0, buddy, h, d).wait_recv()
+            og[1, f, h] = o_buf[buddy, h]
+        for j in range(2):
+            for h in range(2):
+                g_copy(0, j, n1, h, SIB).wait_recv()
+                g_relay(j, h).start()
+                if j == 0:
+                    start(g_first(1, h))
+        g_bulk(2, g_send).wait_recv()
+        for i in (1, 0):
+            hid_copy(i, slot).wait_recv()
+            for k in range(3):
+                a_copy(k, i).start()
+        hall[f] = hidden[slot, seq(f)]
 
     parts = [(s, h) for s in chunks for h in range(2)]
 
     def half_copy(s, h):
         return remote(
-            half_out.at[s, h], half_in.at[s, h], half_send.at[s, h], half_recv.at[s, h], SIB
+            half_out.at[s, h], half_in.at[s, h], half_send.at[0], half_recv.at[s, h], SIB
         )
 
     def piece_copy(s, h, d, target):
         return remote(
             piece_out.at[s, h, d - 1], piece_in.at[s, h, d - 1],
-            piece_send.at[s, h, d - 1], piece_recv.at[s, h, d - 1], {"fs": target},
+            piece_send.at[0], piece_recv.at[s, h], {"fs": target},
         )
 
     def produce(t):
         s, h = parts[t]
-        if 2 <= t < 6:
+        if 4 <= t < 6:
             @pl.when(outer)
             def _():
                 for d in range(2):
@@ -1184,56 +1261,98 @@
             piece_copy(s, h, d, to).start()
         piece_own[s, h] = half_own[s, h, f] + half_in[s, h, f].astype(F32)
 
+    def store(t, total):
+        s, h = parts[t]
+        at = pl.ds(pl.multiple_of((2 * s + h) * nc, nc), nc)
+        out_ref[:, at] = total.astype(BF)
+
     def finish(t):
         s, h = parts[t]
         total = piece_own[s, h]
+        remote(
+            piece_out.at[s, h], piece_in.at[s, h], piece_send.at[0], piece_recv.at[s, h], SIB
+        ).wait_recv()
         for d in range(1, fs):
-            piece_copy(s, h, d, f).wait_recv()
             total += piece_in[s, h, d - 1].astype(F32)
-        at = pl.ds(pl.multiple_of((2 * s + h) * nc, nc), nc)
-        out_ref[:, at] = total.astype(BF)
-        pltpu.make_async_copy(out_ref.at[:, at], out_hbm.at[:, at], out_sem.at[t]).start()
-
-    produce(0)
-    for t in range(1, 2 * sp):
-        produce(t)
-        combine(t - 1)
-    combine(2 * sp - 1)
-    for t in range(2 * sp):
-        finish(t)
-    for t, (s, h) in enumerate(parts):
-        at = pl.ds(pl.multiple_of((2 * s + h) * nc, nc), nc)
-        pltpu.make_async_copy(out_ref.at[:, at], out_hbm.at[:, at], out_sem.at[t]).wait()
-        half_copy(s, h).wait_send()
-        for d in range(1, fs):
-            piece_copy(s, h, d, f).wait_send()
-
-    for kind in range(4):
-        w_copy(kind, me).wait_send()
-    for h, d in quarters:
-        o_copy(0, me, h, d).wait_send()
+        store(t, total)
+
+    def whole_copy(s, h):
+        return remote(
+            half_out.at[s, h, 0], half_in.at[s, h, 0], half_send.at[1], half_recv.at[s, h], SIB
+        )
+
+    def produce_whole(t):
+        s, h = parts[t]
+        total = nn(hall[0], og[t // 2, 0, h])
+        for g in range(1, fs):
+            total += nn(hall[g], og[t // 2, g, h])
+        lo, hi = total[:own], total[own:]
+        half_out[s, h, 0] = jnp.where(c == 0, hi, lo).astype(BF)
+        half_own[s, h, 0] = jnp.where(c == 0, lo, hi)
+        whole_copy(s, h).start()
+
+    def finish_whole(t):
+        s, h = parts[t]
+        whole_copy(s, h).wait_recv()
+        store(t, half_own[s, h, 0] + half_in[s, h, 0].astype(F32))
+
+    def tail_sent(n):
+        ref = half_out.at[pl.ds(0, n)]
+        remote(ref, ref, half_send.at[0], half_recv.at[0, 0], SIB).wait_send()
+        ref = piece_out.at[pl.ds(0, n)]
+        remote(ref, ref, piece_send.at[0], piece_recv.at[0, 0], SIB).wait_send()
+
+    @pl.when(inner)
+    def _():
+        produce(0)
+        for t in range(1, 2 * sp):
+            produce(t)
+            combine(t - 1)
+            if t == 2:
+                o_relay(1, third, 1)
+        combine(2 * sp - 1)
+        for t in range(2 * sp):
+            finish(t)
+        tail_sent(sp)
 
     @pl.when(outer)
     def _():
-        for h in range(2):
-            x_out(h).wait_send()
+        produce(4)
+        combine(4)
+        a_bulk().wait_recv()
+        for t in range(4):
+            produce_whole(t)
+        for t in range(4):
+            finish_whole(t)
+        for t in range(5, 2 * sp):
+            produce(t)
+            combine(t)
+        for t in range(4, 2 * sp):
+            finish(t)
+        tail_sent(sp // 2)
+        ref = half_out.at[0, 0]
+        remote(ref, ref, half_send.at[1], half_recv.at[0, 0], SIB).wait_send()
+        g_bulk(3, g_send).wait_send()
+        a_bulk().wait_send()
+
+    @pl.when(outer)
+    def _():
+        x_bulk(slot, 2).wait_send()
+        for kind in range(4):
+            w_bulk(kind, 1).wait_send()
+        o_bulk(0, 1).wait_send()
 
     @pl.when(inner)
     def _():
         for s in range(2):
-            for copy in x_all(s, 0) + x_all(s, 1):
-                copy.wait_send()
+            x_bulk(s, 14).wait_send()
+        l_bulk(7, 0).wait_send()
         for kind in range(4):
-            w_copy(kind, buddy).wait_send()
-        for copy in l_first() + l_onward():
-            copy.wait_send()
-        for s in chunks[1:]:
-            kv_share(s, side).wait_send()
-            low_share(s, c).wait_send()
-        for h, d in quarters:
-            o_copy(0, buddy, h, d).wait_send()
-            for s in (me, third, fourth):
-                o_copy(1, s, h, d).wait_send()
+            w_bulk(kind, 2).wait_send()
+        share_bulk(0).wait_send()
+        share_bulk(1).wait_send()
+        o_bulk(0, 2).wait_send()
+        o_bulk(1, 3).wait_send()
         for i in range(2):
             hid_copy(i, far_slot).wait_send()
 
@@ -1264,7 +1383,6 @@
     scratch = [
         vm((own, d), BF),
         *(vm(shape, dtype) for shape, dtype in small),
-        vm((own, sp * nc), BF),
         vm((2, all_rows, d), BF),
         vm((d, 2 * pair), BF),
         vm((d, VALUE_DIM + pair), BF),
@@ -1276,6 +1394,9 @@
         vm((2, all_rows, VALUE_DIM), BF),
         vm((2, all_rows, pair), F32),
         vm((2, all_rows, 2 * pair), F32),
+        vm((2, all_rows, VALUE_DIM + pair), F32),
+        vm((2, fs, 2, depth, nc // 2), BF),
+        vm((fs, rows, depth), BF),
         vm((fs * tp, rank, 2 * own), BF),
         vm((2 * WINDOW, 2 * WINDOW), F32),
         vm((fs, 2 * WINDOW, 2 * WINDOW), F32),
@@ -1294,33 +1415,38 @@
         vm((sp, 2, fs - 1, own, nc // 2), BF),
         vm((sp, 2, fs - 1, own, nc // 2), BF),
         vm((sp, 2, own, nc // 2), F32),
-        dma((17,)),
-        dma((2 * sp,)),
-        dma((7,)),
-        dma((fs * tp,)),
-        dma((2, 7, 2)),
-        dma((2, fs * tp, 2)),
+        dma((11,)),
+        dma((1,)),
+        dma((2,)),
+        dma((2,)),
+        dma((2, 4, 2)),
+        dma((2,)),
+        dma((4,)),
         dma((4, sp)),
-        dma((4, sp)),
-        dma((2, sp)),
-        dma((2, sp)),
-        dma((2, sp, 2, 2)),
+        dma((2,)),
+        dma((sp + 1,)),
+        dma((2,)),
         dma((sp, 2, 2)),
         dma((4,)),
         dma((2,)),
         dma((2,)),
         dma((2,)),
+        dma((2,)),
         dma((sp, 2)),
+        dma((1,)),
         dma((sp, 2)),
-        dma((sp, 2, fs - 1)),
-        dma((sp, 2, fs - 1)),
+        dma((1,)),
+        dma((2, 2)),
+        dma((1,)),
+        dma((1,)),
+        dma((1,)),
     ]
     anywhere = pl.BlockSpec(memory_space=pl.ANY)
     return pl.pallas_call(
         functools.partial(fold_kernel, sizes),
-        out_shape=jax.ShapeDtypeStruct((own, sp * nc), BF),
+        out_shape=pltpu.VMEM((own, sp * nc), BF),
         in_specs=[anywhere] * 15,
-        out_specs=anywhere,
+        out_specs=pl.BlockSpec(memory_space=pltpu.VMEM),
         scratch_shapes=scratch,
         compiler_params=pltpu.CompilerParams(
             has_side_effects=True, vmem_limit_bytes=60 * 1024 * 1024, collective_id=0

time: 58.3 us -> 53.8 us (0.923)
  Pallas kernels: 56.4 us -> 52.9 us
  local copies, waits for them, and re-layouts: 1.67 us -> 0.71 us
    pallas_call x1, Pallas kernels: 56.4 us -> 52.9 us  [fold_call(): pl.pallas_call(functools.partial(fold_kernel, sizes), out_shape=pltpu.VME...]
    unnamed x1, local copies, waits for them, and re-layouts: 1.67 us -> 0.71 us
where the time goes in v4:
time: 53.8 us; the launch traced here: 53.6 us
  Pallas kernels  52.9 us (98%)
  local copies, waits for them, and re-layouts  0.71 us (1%)
    pallas_call x1, Pallas kernels, fold_call(): pl.pallas_call(functools.partial(fold_kernel, sizes), out_shape=pltpu.VME...  52.9 us

profile of v4, /device:TPU:0, one launch (start us, length us, event | category | flops | bytes accessed | tf_op | source)
XLA Modules:
  0.0 53.6 jit_solution(17417593303615515072)
XLA Ops:
  0.0 52.9 %shard_map.145 = bf16[64,2048]{1,0:T(8,128)(2,1)S(1)} custom-call(bf16[64,2048]{1,0:T(8,128)(2,1)} %bitcast.8, bf16[512,512]{1,0:T(8,128)(2,1)} %gv_ref.1, bf16[512,512]{1,0:T(8,128)(2,1)} %wq_ref.1, bf16[512,256]{1,0:T(8,128)(2,1)} %gq_ref.1, bf16[512,256]{1,0:T(8,128)(2,1)} %gk_ref.1, bf16[512,128]{1,0:T(8,128)(2,1)} %wk_ref.1, bf16[512,128]{1,0:T(8,128)(2,1)} %wv_ref.1, ...), custom_call_target="tpu_custom_call" | custom-call | tf_op jit(solution)/shard_map/pallas_call | solution.py:1445
  52.9 0.7 %copy.17 = bf16[1,64,2048]{2,1,0:T(8,128)(2,1)} copy(bf16[1,64,2048]{2,1,0:T(8,128)(2,1)S(1)} %bitcast.7) | data formatting | bytes 524288

commit v5 on v4

--- a/solution.py
+++ b/solution.py
@@ -707,7 +707,7 @@
         copy.start()
 
     mine = f * tp + c
-    b1, b2, b3 = n1 * tp + c, n2 * tp + c, (fs - 1 - f) * tp + c
+    b1, b2, b3 = xn * tp + c, yn * tp + c, (fs - 1 - f) * tp + c
 
     for copy in locals_[11:]:
         copy.wait()
@@ -732,15 +732,16 @@
 
     SIB = {"tp": 1 - c}
 
-    def x_first(s, h):
+    def ways(far, h):
+        return (xn, yn) if far and h == 1 else (n1, n2)
+
+    def x_first(s, h, far):
+        w1, w2 = ways(far, h)
         return [
-            x_copy(s, mine, h, {"fs": n1}, 1),
-            x_copy(s, mine, h, {"fs": n2}, 2),
+            x_copy(s, mine, h, {"fs": w1}, 1),
+            x_copy(s, mine, h, {"fs": w2}, 2),
             x_sib(s, mine, h),
         ]
-
-    def x_from1(s, h):
-        return [x_copy(s, b1, h, {"fs": n2}, 3), x_sib(s, b1, h)]
 
     def x_out(h):
         return x_copy(slot, mine, h, {"sp": middle}, 0)
@@ -789,10 +790,13 @@
         ref = o_buf.at[pl.ds(0, n)]
         return remote(ref, ref, o_send.at[way], o_recv.at[0, 0, 0], {"sp": middle})
 
+    def o_part(way, s, h, d):
+        o_copy(0, s, h, d).wait_recv()
+        o_copy(way, s, h, d).start()
+
     def o_relay(way, s, h):
         for d in range(2):
-            o_copy(0, s, h, d).wait_recv()
-            o_copy(way, s, h, d).start()
+            o_part(way, s, h, d)
 
     quarters = [(h, d) for h in range(2) for d in range(2)]
 
@@ -827,7 +831,7 @@
     @pl.when(inner)
     def _():
         for h in range(2):
-            start(x_first(slot, h))
+            start(x_first(slot, h, False))
 
     local_wait(tiles, 0)
     for copy in locals_[4:6]:
@@ -902,11 +906,14 @@
             if kind == KV:
                 kv_share(s, side).start()
 
-        def neighbours(s, h):
-            x_copy(s, b1, h, SIB, 1).wait_recv()
-            start(x_from1(s, h))
-            x_copy(s, b2, h, SIB, 2).wait_recv()
-            x_sib(s, b2, h).start()
+        def neighbours(s, h, far):
+            w1, w2 = ways(far, h)
+            i1, i2 = w1 * tp + c, w2 * tp + c
+            x_copy(s, i1, h, SIB, 1).wait_recv()
+            x_copy(s, i1, h, {"fs": w2}, 3).start()
+            x_sib(s, i1, h).start()
+            x_copy(s, i2, h, SIB, 2).wait_recv()
+            x_sib(s, i2, h).start()
 
         def corner(s):
             for h in range(2):
@@ -1007,23 +1014,23 @@
 
         def far_rows(h):
             x_copy(far_slot, mine, h, SIB, 0).wait_recv()
-            start(x_first(far_slot, h))
+            start(x_first(far_slot, h, True))
 
         arrive(LOW, buddy, True)
         w_copy(STATE, me).start()
         o_copy(0, me, 0, 0).start()
         arrive(LOW, third, False)
         arrive(KV, third, False)
-        neighbours(slot, 0)
+        neighbours(slot, 0, False)
         far_rows(0)
         arrive(LOW, fourth, False)
-        neighbours(slot, 1)
+        neighbours(slot, 1, False)
         far_rows(1)
         share_bulk(1).wait_recv()
         own_low()
         start(l_first())
         arrive(KV, buddy, True)
-        neighbours(far_slot, 0)
+        neighbours(far_slot, 0, True)
         arrive(QUERY, buddy, True)
         o_copy(0, me, 0, 1).start()
         corner(slot)
@@ -1031,7 +1038,7 @@
         arrive(QUERY, third, False)
         kv_share(third, 1 - side).wait_recv()
         acc[slot] = window_maps(slot, (me, third))
-        neighbours(far_slot, 1)
+        neighbours(far_slot, 1, True)
         arrive(STATE, buddy, True)
         arrive(KV, fourth, False)
         l_bulk(3, 0).wait_recv()
@@ -1052,11 +1059,8 @@
         def _():
             edge.start()
 
-        o_copy(0, me, 1, 0).start()
-
-        @pl.when(me > 1)
-        def _():
-            o_copy(0, me, 1, 1).start()
+        for d in range(2):
+            o_copy(0, me, 1, d).start()
 
         siblings(far_slot)
         place(far_slot, window_maps(far_slot, chunks))
@@ -1084,6 +1088,12 @@
 
         window(far_slot)
         hid_copy(1, far_slot).start()
+
+        @pl.when(me > 1)
+        def _():
+            for h in range(2):
+                o_relay(0, buddy, h)
+
         acc2[far_slot] = state_maps(far_slot, chunks[:3])
 
         @pl.when(me > 1)
@@ -1116,6 +1126,7 @@
         @pl.when(me == 1)
         def _():
             state.start()
+            o_relay(0, buddy, 0)
 
         for s in range(2):
             for p in range(fs // 2):
@@ -1133,16 +1144,18 @@
                     ).astype(BF)
                     local_out[s, seq(2 * p + j)] = nn(scores, gvb[s, seq(2 * p + j)])
                     q_far[s, seq(2 * p + j)] = jnp.where(here, qf, 0.0).astype(BF)
+            if s == 0:
+                @pl.when(me == 1)
+                def _():
+                    o_relay(1, third, 1)
 
         @pl.when(me == 1)
         def _():
-            o_copy(0, me, 1, 1).start()
-
-        for h in range(2):
-            o_relay(0, buddy, h)
+            o_relay(0, buddy, 1)
 
         @pl.when(me > 1)
         def _():
+            o_relay(1, third, 1)
             edge_share(1 - side).wait_recv()
             window(slot)
             state.wait_recv()
@@ -1223,7 +1236,10 @@
             half_out.at[s, h], half_in.at[s, h], half_send.at[0], half_recv.at[s, h], SIB
         )
 
-    def piece_copy(s, h, d, target):
+    peers = (corner_f, n1, n2)
+
+    def piece_copy(s, h, d):
+        target = peers[d - 1]
         return remote(
             piece_out.at[s, h, d - 1], piece_in.at[s, h, d - 1],
             piece_send.at[0], piece_recv.at[s, h], {"fs": target},
@@ -1237,12 +1253,10 @@
                 for d in range(2):
                     o_copy(0, s, h, d).wait_recv()
         if t >= 6:
-            for d in range(2):
-                o_copy(0, s, h, d).wait_recv()
-
-                @pl.when(inner)
-                def _():
-                    o_copy(1, s, h, d).start()
+            @pl.when(outer)
+            def _():
+                for d in range(2):
+                    o_copy(0, s, h, d).wait_recv()
 
         w = o_buf[s, h]
         for b in range(fs):
@@ -1256,9 +1270,9 @@
         s, h = parts[t]
         half_copy(s, h).wait_recv()
         for d in range(1, fs):
-            to = lax.rem(f + d, fs)
+            to = peers[d - 1]
             piece_out[s, h, d - 1] = (half_own[s, h, to] + half_in[s, h, to].astype(F32)).astype(BF)
-            piece_copy(s, h, d, to).start()
+            piece_copy(s, h, d).start()
         piece_own[s, h] = half_own[s, h, f] + half_in[s, h, f].astype(F32)
 
     def store(t, total):
@@ -1308,8 +1322,8 @@
         for t in range(1, 2 * sp):
             produce(t)
             combine(t - 1)
-            if t == 2:
-                o_relay(1, third, 1)
+            for h, d in {2: quarters[:2], 4: quarters[2:3], 5: quarters[3:]}.get(t, ()):
+                o_part(1, fourth, h, d)
         combine(2 * sp - 1)
         for t in range(2 * sp):
             finish(t)
@@ -1318,15 +1332,18 @@
     @pl.when(outer)
     def _():
         produce(4)
+        produce(5)
         combine(4)
         a_bulk().wait_recv()
         for t in range(4):
             produce_whole(t)
+        combine(5)
+        produce(6)
+        produce(7)
+        combine(6)
+        combine(7)
         for t in range(4):
             finish_whole(t)
-        for t in range(5, 2 * sp):
-            produce(t)
-            combine(t)
         for t in range(4, 2 * sp):
             finish(t)
         tail_sent(sp // 2)

time: 53.8 us -> 53.5 us (level)
  no operation moved by 1% of the time
where the time goes in v5:
time: 53.5 us; the launch traced here: 53.3 us
  Pallas kernels  52.6 us (98%)
  local copies, waits for them, and re-layouts  0.71 us (1%)
    pallas_call x1, Pallas kernels, fold_call(): pl.pallas_call(functools.partial(fold_kernel, sizes), out_shape=pltpu.VME...  52.6 us

profile of v5, /device:TPU:0, one launch (start us, length us, event | category | flops | bytes accessed | tf_op | source)
XLA Modules:
  0.0 53.3 jit_solution(15069016468804457907)
XLA Ops:
  0.0 52.6 %shard_map.145 = bf16[64,2048]{1,0:T(8,128)(2,1)S(1)} custom-call(bf16[64,2048]{1,0:T(8,128)(2,1)} %bitcast.8, bf16[512,512]{1,0:T(8,128)(2,1)} %gv_ref.1, bf16[512,512]{1,0:T(8,128)(2,1)} %wq_ref.1, bf16[512,256]{1,0:T(8,128)(2,1)} %gq_ref.1, bf16[512,256]{1,0:T(8,128)(2,1)} %gk_ref.1, bf16[512,128]{1,0:T(8,128)(2,1)} %wk_ref.1, bf16[512,128]{1,0:T(8,128)(2,1)} %wv_ref.1, ...), custom_call_target="tpu_custom_call" | custom-call | tf_op jit(solution)/shard_map/pallas_call | solution.py:1462
  52.6 0.7 %copy.17 = bf16[1,64,2048]{2,1,0:T(8,128)(2,1)} copy(bf16[1,64,2048]{2,1,0:T(8,128)(2,1)S(1)} %bitcast.7) | data formatting | bytes 524288

commit v6 on v5

--- a/solution.py
+++ b/solution.py
@@ -1334,13 +1334,13 @@
         produce(4)
         produce(5)
         combine(4)
+        combine(5)
+        produce(6)
         a_bulk().wait_recv()
         for t in range(4):
             produce_whole(t)
-        combine(5)
-        produce(6)
+        combine(6)
         produce(7)
-        combine(6)
         combine(7)
         for t in range(4):
             finish_whole(t)

time: 53.5 us -> 53 us (level)
    pallas_call x1, Pallas kernels: 52.6 us -> 52.1 us  [fold_call(): pl.pallas_call(functools.partial(fold_kernel, sizes), out_shape=pltpu.VME...]
where the time goes in v6:
time: 53 us; the launch traced here: 52.8 us
  Pallas kernels  52.1 us (98%)
  local copies, waits for them, and re-layouts  0.71 us (1%)
    pallas_call x1, Pallas kernels, fold_call(): pl.pallas_call(functools.partial(fold_kernel, sizes), out_shape=pltpu.VME...  52.1 us

profile of v6, /device:TPU:0, one launch (start us, length us, event | category | flops | bytes accessed | tf_op | source)
XLA Modules:
  0.0 52.8 jit_solution(16550308267059989279)
XLA Ops:
  0.0 52.1 %shard_map.145 = bf16[64,2048]{1,0:T(8,128)(2,1)S(1)} custom-call(bf16[64,2048]{1,0:T(8,128)(2,1)} %bitcast.8, bf16[512,512]{1,0:T(8,128)(2,1)} %gv_ref.1, bf16[512,512]{1,0:T(8,128)(2,1)} %wq_ref.1, bf16[512,256]{1,0:T(8,128)(2,1)} %gq_ref.1, bf16[512,256]{1,0:T(8,128)(2,1)} %gk_ref.1, bf16[512,128]{1,0:T(8,128)(2,1)} %wk_ref.1, bf16[512,128]{1,0:T(8,128)(2,1)} %wv_ref.1, ...), custom_call_target="tpu_custom_call" | custom-call | tf_op jit(solution)/shard_map/pallas_call | solution.py:1462
  52.1 0.7 %copy.17 = bf16[1,64,2048]{2,1,0:T(8,128)(2,1)} copy(bf16[1,64,2048]{2,1,0:T(8,128)(2,1)S(1)} %bitcast.7) | data formatting | bytes 524288
